TPU v7x, 32 devices: a whole 2x2x4 slice. The times are simulated.
32 devices in a mesh: ep: 8 (over z, y), tp: 4 (over x, core).
Axes of the slice: x: 2, y: 2, z: 4, core: 2. Of those that a mesh axis runs over, the one named last changes fastest.
Arguments:
- hidden_in: bfloat16 [384, 2048], P('ep'), may hold values from -6 to 6
- carried_state: float32 [384, 4, 128, 256], P('ep', 'tp'), may hold values from -6 to 6
- input_gain: bfloat16 [2048], replicated, may hold values from 0.099609375 to 1.8984375
- query_weight: bfloat16 [2048, 512], P(None, 'tp'), may hold values from -0.125 to 0.125
- key_weight: bfloat16 [2048, 512], P(None, 'tp'), may hold values from -0.125 to 0.125
- value_weight: bfloat16 [2048, 1024], P(None, 'tp'), may hold values from -0.125 to 0.125
- outgate_weight: bfloat16 [2048, 1024], P(None, 'tp'), may hold values from -0.125 to 0.125
- decay_weight: bfloat16 [2048, 512], P(None, 'tp'), may hold values from -0.5 to 0.5
- decay_shift: float32 [384, 512], P('ep', 'tp'), may hold values from -0.7 to 0
- head_gain: bfloat16 [4, 256], P('tp'), may hold values from 0.099609375 to 1.8984375
- output_weight: bfloat16 [1024, 2048], P('tp'), may hold values from -0.1875 to 0.1875
- channel_gain: bfloat16 [2048], replicated, may hold values from 0.099609375 to 1.8984375
- branch_gate: bfloat16 [2048], replicated, may hold values from -0.125 to 0.125
- routes: int32 [384, 2], P('ep'), may hold values from 0 to 7, all different within a row; in each aligned block of 48 rows (0 to 47, 48 to 95, ...) at most 14 rows name the same one
- route_weights: float32 [384, 2], P('ep'), may hold values from 0.1 to 1
- expert_gate: bfloat16 [8, 2048, 3072], P('ep', None, 'tp'), may hold values from -0.125 to 0.125
- expert_up: bfloat16 [8, 2048, 3072], P('ep', None, 'tp'), may hold values from -0.125 to 0.125
- expert_down: bfloat16 [8, 3072, 2048], P('ep', 'tp'), may hold values from -0.109375 to 0.109375
- dense_gate: bfloat16 [2048, 4096], P('tp', 'ep'), may hold values from -0.125 to 0.125
- dense_up: bfloat16 [2048, 4096], P('tp', 'ep'), may hold values from -0.125 to 0.125
- dense_down: bfloat16 [4096, 2048], P('ep', 'tp'), may hold values from -0.09375 to 0.09375
Outputs:
- mixed: bfloat16 [384, 2048], P('ep', 'tp')
- new_state: float32 [384, 4, 128, 256], P('ep', 'tp')
Inputs may be any that keep to these rules, and one draw needn't show every extreme that they name: `routes`: each row names 2 different experts. Among the rows of one index of ep no expert is named more than 14 times, and in every draw some expert is named exactly 14 times by the rows of some index.
All inputs are finite; a program needn't handle non-finite values.
Results may differ from a plain program's by a relative error of at most 0.02.
Values may be sent and summed in bfloat16 or wider, within the bound.
A program may use at most 128 MiB of HBM per device.

v0:
```python
import functools

import jax
import jax.numpy as jnp
from jax import lax
from jax.experimental import pallas as pl
from jax.experimental.pallas import tpu as pltpu
from jax.sharding import PartitionSpec as P

EPSILON = 1e-06
TAU_DECAY = 16.0
MESH = pl.DeviceIdType.MESH


def rms_factor(values):
    return lax.rsqrt(jnp.mean(values * values, axis=-1, keepdims=True) + EPSILON)


def matmul(left, right):
    return jnp.dot(left, right, preferred_element_type=jnp.float32)


def silu(values):
    return values * jax.nn.sigmoid(values)


def layer_kernel(
    n_ep,
    n_tp,
    gated_ref,
    outw_ref,
    hid_ref,
    gain_ref,
    gate_ref,
    sel_ref,
    comb_hi_ref,
    comb_lo_ref,
    eg_hbm,
    eu_hbm,
    ed_hbm,
    dg_hbm,
    du_hbm,
    dd_hbm,
    mixed_ref,
    eg,
    eu,
    ed,
    dgw,
    duw,
    ddw,
    sel_recv,
    p_send,
    p_recv,
    st_send,
    st_recv,
    mid_buf,
    br_buf,
    piece,
    rows_all,
    g_send,
    g_recv,
    u_send,
    u_recv,
    e_hid,
    eo_send,
    eo_recv,
    d_hid,
    out_send,
    out_recv,
    ret_send,
    ret,
    w_sem,
    tp_ssem,
    tp_rsem,
    ep_ssem,
    ep_rsem,
):
    f32, bf16 = jnp.float32, jnp.bfloat16
    ep = lax.axis_index("ep")
    tp = lax.axis_index("tp")
    tokens, width = hid_ref.shape
    quarter = width // n_tp
    own = pl.ds(pl.multiple_of(tp * quarter, quarter), quarter)
    cap = sel_ref.shape[1]

    loads = []
    for i, (src, dst) in enumerate(
        ((dg_hbm, dgw), (du_hbm, duw), (eg_hbm, eg), (eu_hbm, eu), (ed_hbm, ed), (dd_hbm, ddw))
    ):
        load = pltpu.make_async_copy(src, dst, w_sem.at[i])
        load.start()
        loads.append(load)

    barrier = pltpu.get_barrier_semaphore()
    for d in range(1, n_tp):
        pl.semaphore_signal(
            barrier, inc=1, device_id=(ep, lax.rem(tp + d, n_tp)), device_id_type=MESH
        )
    for d in range(1, n_ep):
        pl.semaphore_signal(
            barrier, inc=1, device_id=(lax.rem(ep + d, n_ep), tp), device_id_type=MESH
        )

    def over_tp(phase, src_of, dst_of):
        copies = []
        for d in range(1, n_tp):
            peer = lax.rem(tp + d, n_tp)
            copy = pltpu.make_async_remote_copy(
                src_ref=src_of(peer),
                dst_ref=dst_of(d),
                send_sem=tp_ssem.at[phase, d - 1],
                recv_sem=tp_rsem.at[phase, d - 1],
                device_id=(ep, peer),
                device_id_type=MESH,
            )
            copy.start()
            copies.append(copy)
        return copies

    def over_ep(phase, src_of, dst_of):
        copies = []
        for d in range(1, n_ep):
            peer = lax.rem(ep + d, n_ep)
            copy = pltpu.make_async_remote_copy(
                src_ref=src_of(peer),
                dst_ref=dst_of(d),
                send_sem=ep_ssem.at[phase, d - 1],
                recv_sem=ep_rsem.at[phase, d - 1],
                device_id=(peer, tp),
                device_id_type=MESH,
            )
            copy.start()
            copies.append(copy)
        return copies

    def spread(axis, phase, buf):
        n, me = (n_tp, tp) if axis == "tp" else (n_ep, ep)
        ssem, rsem = (tp_ssem, tp_rsem) if axis == "tp" else (ep_ssem, ep_rsem)
        near = me + 1 - 2 * lax.rem(me, 2)
        half = n // 2

        def send(index, block, peer):
            copy = pltpu.make_async_remote_copy(
                src_ref=buf.at[block],
                dst_ref=buf.at[block],
                send_sem=ssem.at[phase, index],
                recv_sem=rsem.at[phase, index],
                device_id=(ep, peer) if axis == "tp" else (peer, tp),
                device_id_type=MESH,
            )
            copy.start()
            return copy

        copies = [send(m - 1, me, lax.rem(me + 2 * m, n)) for m in range(1, half)]
        copies.append(send(half - 1, me, near))
        for m in range(1, half):
            copies[m - 1].wait_recv()
            source = lax.rem(me - 2 * m + n, n)
            copies.append(send(half - 1 + m, source, near))
            yield source
        copies[half - 1].wait_recv()
        yield near
        for m in range(1, half):
            copies[half - 1 + m].wait_recv()
            yield lax.rem(near - 2 * m + n, n)
        sent.append(copies)

    sent = []

    def arrive(copies):
        for copy in copies:
            copy.wait_recv()

    for j in range(n_tp):
        p_send[j] = matmul(gated_ref[...], outw_ref[:, j * quarter : (j + 1) * quarter]).astype(bf16)
    pl.semaphore_wait(barrier, n_tp + n_ep - 2)
    c_part = over_tp(0, lambda peer: p_send.at[peer], lambda d: p_recv.at[d - 1])
    c_sel = over_ep(0, lambda peer: sel_ref.at[peer], lambda d: sel_recv.at[ep])
    sel_recv[ep] = sel_ref[ep]
    attended = p_send[tp].astype(f32)
    for d in range(1, n_tp):
        c_part[d - 1].wait_recv()
        attended = attended + p_recv[d - 1].astype(f32)
    middle = (hid_ref[:, own].astype(f32) + attended).astype(bf16).astype(f32)
    gain = gain_ref[:, own].astype(f32)
    squares = jnp.sum(middle * middle, axis=-1, keepdims=True)
    inner = jnp.sum(middle * gain * gate_ref[:, own].astype(f32), axis=-1, keepdims=True)
    lane = lax.broadcasted_iota(jnp.int32, (tokens, 128), 1)
    st_send[...] = jnp.where(lane < 64, squares, inner)
    c_stat = over_tp(1, lambda peer: st_send, lambda d: st_recv.at[d - 1])
    mid_buf[...] = middle
    totals = st_send[...]
    for d in range(1, n_tp):
        c_stat[d - 1].wait_recv()
        totals = totals + st_recv[d - 1]
    factor = lax.rsqrt(totals[:, 0:1] / width + EPSILON)
    br_buf[...] = jnp.broadcast_to(jax.nn.sigmoid(totals[:, 64:65] * factor), (tokens, 128))
    piece[ep] = (middle * factor * gain).astype(bf16)

    arrive(c_sel)

    def pick(source):
        picked = matmul(sel_recv[source][:, :tokens], piece[source]).astype(bf16)
        rows_all[tp, pl.ds(pl.multiple_of(source * cap, cap), cap), :] = picked

    pieces = spread("ep", 1, piece)
    first = next(pieces)
    pick(ep)
    pick(first)
    for source in pieces:
        pick(source)
    rows = spread("tp", 2, rows_all)
    loads[0].wait()
    loads[1].wait()
    everyone = piece[...].reshape(n_ep * tokens, quarter)
    units = dgw.shape[1]
    share = n_ep * tokens // n_tp
    next(rows)
    g_send[...] = matmul(everyone, dgw[...]).astype(bf16).reshape(n_tp, share, units)
    c_g = over_tp(3, lambda peer: g_send.at[peer], lambda d: g_recv.at[d - 1])
    u_send[...] = matmul(everyone, duw[...]).astype(bf16).reshape(n_tp, share, units)
    c_u = over_tp(4, lambda peer: u_send.at[peer], lambda d: u_recv.at[d - 1])

    loads[2].wait()
    loads[3].wait()
    for _ in rows:
        pass
    block = eg.shape[1]
    tile = 256 if block % 256 == 0 else 128

    @pl.loop(0, block // tile)
    def _(i):
        cols = pl.ds(pl.multiple_of(i * tile, tile), tile)
        gate_part = matmul(rows_all[0], eg[0:quarter, cols])
        up_part = matmul(rows_all[0], eu[0:quarter, cols])
        for j in range(1, n_tp):
            span = slice(j * quarter, (j + 1) * quarter)
            gate_part = gate_part + matmul(rows_all[j], eg[span, cols])
            up_part = up_part + matmul(rows_all[j], eu[span, cols])
        e_hid[:, cols] = (silu(gate_part) * up_part).astype(bf16)

    g_sum = g_send[tp].astype(f32)
    u_sum = u_send[tp].astype(f32)
    for d in range(1, n_tp):
        c_g[d - 1].wait_recv()
        g_sum = g_sum + g_recv[d - 1].astype(f32)
    for d in range(1, n_tp):
        c_u[d - 1].wait_recv()
        u_sum = u_sum + u_recv[d - 1].astype(f32)
    d_hid[tp] = (silu(g_sum) * u_sum).astype(bf16)
    held = spread("tp", 5, d_hid)
    next(held)

    loads[4].wait()
    for j in range(n_tp):
        eo_send[j] = matmul(e_hid[...], ed[:, j * quarter : (j + 1) * quarter]).astype(bf16)
    c_eo = over_tp(6, lambda peer: eo_send.at[peer], lambda d: eo_recv.at[d - 1])

    loads[5].wait()
    for _ in held:
        pass
    hidden = d_hid[...].reshape(n_ep * tokens, units)
    out_send[...] = matmul(hidden, ddw[...]).astype(bf16).reshape(n_ep, tokens, quarter)
    c_out = over_ep(2, lambda peer: out_send.at[peer], lambda d: out_recv.at[d - 1])

    summed = eo_send[tp].astype(f32)
    for d in range(1, n_tp):
        c_eo[d - 1].wait_recv()
        summed = summed + eo_recv[d - 1].astype(f32)
    ret_send[...] = summed.astype(bf16).reshape(n_ep, cap, quarter)
    c_ret = over_ep(3, lambda peer: ret_send.at[peer], lambda d: ret.at[ep])
    ret[ep] = ret_send[ep]

    dense = out_send[ep].astype(f32)
    for d in range(1, n_ep):
        c_out[d - 1].wait_recv()
        dense = dense + out_recv[d - 1].astype(f32)
    arrive(c_ret)
    answers = ret[...].reshape(n_ep * cap, quarter)
    routed = matmul(comb_hi_ref[...], answers) + matmul(comb_lo_ref[...], answers)
    mixed_ref[...] = (mid_buf[...] + br_buf[:, 0:1] * dense + routed).astype(bf16)

    for copies in (c_part, c_sel, c_stat, c_g, c_u, c_eo, c_out, c_ret, *sent):
        for copy in copies:
            copy.wait_send()


def run_layer(gated, output_weight, hid, gain, gate, sel, comb_hi, comb_lo, eg, eu, ed, dg, du, dd):
    n_ep, n_tp = lax.axis_size("ep"), lax.axis_size("tp")
    tokens = hid.shape[0]
    quarter = hid.shape[1] // n_tp
    cap = sel.shape[1]
    items = n_ep * cap
    share = n_ep * tokens // n_tp
    units = dg.shape[1]
    bf16, f32 = jnp.bfloat16, jnp.float32
    vmem = pl.BlockSpec(memory_space=pltpu.VMEM)
    anyspace = pl.BlockSpec(memory_space=pl.ANY)
    scratch = [pltpu.VMEM(w.shape, bf16) for w in (eg, eu, ed, dg, du, dd)]
    scratch += [
        pltpu.VMEM(sel.shape, bf16),
        pltpu.VMEM((n_tp, tokens, quarter), bf16),
        pltpu.VMEM((n_tp - 1, tokens, quarter), bf16),
        pltpu.VMEM((tokens, 128), f32),
        pltpu.VMEM((n_tp - 1, tokens, 128), f32),
        pltpu.VMEM((tokens, quarter), f32),
        pltpu.VMEM((tokens, 128), f32),
        pltpu.VMEM((n_ep, tokens, quarter), bf16),
        pltpu.VMEM((n_tp, items, quarter), bf16),
        pltpu.VMEM((n_tp, share, units), bf16),
        pltpu.VMEM((n_tp - 1, share, units), bf16),
        pltpu.VMEM((n_tp, share, units), bf16),
        pltpu.VMEM((n_tp - 1, share, units), bf16),
        pltpu.VMEM((items, eg.shape[1]), bf16),
        pltpu.VMEM((n_tp, items, quarter), bf16),
        pltpu.VMEM((n_tp - 1, items, quarter), bf16),
        pltpu.VMEM((n_tp, share, units), bf16),
        pltpu.VMEM((n_ep, tokens, quarter), bf16),
        pltpu.VMEM((n_ep - 1, tokens, quarter), bf16),
        pltpu.VMEM((n_ep, cap, quarter), bf16),
        pltpu.VMEM((n_ep, cap, quarter), bf16),
        pltpu.SemaphoreType.DMA((6,)),
        pltpu.SemaphoreType.DMA((7, n_tp - 1)),
        pltpu.SemaphoreType.DMA((7, n_tp - 1)),
        pltpu.SemaphoreType.DMA((4, n_ep - 1)),
        pltpu.SemaphoreType.DMA((4, n_ep - 1)),
    ]
    return pl.pallas_call(
        functools.partial(layer_kernel, n_ep, n_tp),
        out_shape=jax.ShapeDtypeStruct((tokens, quarter), bf16),
        in_specs=[vmem] * 8 + [anyspace] * 6,
        out_specs=vmem,
        scratch_shapes=scratch,
        compiler_params=pltpu.CompilerParams(
            collective_id=0, has_side_effects=True, vmem_limit_bytes=60 * 1024 * 1024
        ),
    )(gated, output_weight, hid, gain, gate, sel, comb_hi, comb_lo, eg, eu, ed, dg, du, dd)


def attention_kernel(
    cap,
    hidden_ref,
    gain_ref,
    shift_ref,
    head_gain_ref,
    routes_ref,
    weights_ref,
    qw_hbm,
    kw_hbm,
    vw_hbm,
    ow_hbm,
    fw_hbm,
    state_hbm,
    gated_ref,
    sel_ref,
    comb_hi_ref,
    comb_lo_ref,
    new_hbm,
    qw,
    kw,
    vw,
    ow,
    fw,
    state,
    query,
    key,
    value,
    decay,
    readout,
    w_sem,
    in_sem,
    out_sem,
):
    f32, bf16 = jnp.float32, jnp.bfloat16
    tokens = hidden_ref.shape[0]
    heads, key_dim, value_dim = state.shape[1:]
    groups = tokens // 8
    loads = []
    pairs = ((fw_hbm, fw), (kw_hbm, kw), (qw_hbm, qw), (vw_hbm, vw), (ow_hbm, ow))
    for i, (src, dst) in enumerate(pairs):
        load = pltpu.make_async_copy(src, dst, w_sem.at[i])
        load.start()
        loads.append(load)

    def fetch(g):
        rows = pl.ds(g * 8, 8)
        return pltpu.make_async_copy(state_hbm.at[rows], state.at[rows], in_sem.at[g])

    def put(g):
        rows = pl.ds(g * 8, 8)
        return pltpu.make_async_copy(state.at[rows], new_hbm.at[rows], out_sem.at[g])

    for g in range(groups):
        fetch(g).start()

    inputs = hidden_ref[...].astype(f32)
    normed = (inputs * rms_factor(inputs) * gain_ref[...].astype(f32)).astype(bf16)

    items = comb_hi_ref.shape[1]
    lane = lax.broadcasted_iota(jnp.int32, (tokens, 128), 1)
    first, second = routes_ref[:, 0:1], routes_ref[:, 1:2]
    chosen0 = jnp.where(lane == first, 1.0, 0.0)
    chosen1 = jnp.where(lane == second, 1.0, 0.0)
    row = lax.broadcasted_iota(jnp.int32, (tokens, tokens), 0)
    col = lax.broadcasted_iota(jnp.int32, (tokens, tokens), 1)
    before = jnp.where(row > col, 1.0, 0.0).astype(bf16)
    earlier = matmul(before, (chosen0 + chosen1).astype(bf16))
    slot0 = jnp.sum(earlier * chosen0, axis=1, keepdims=True)
    slot1 = jnp.sum(earlier * chosen1, axis=1, keepdims=True)
    table = lax.broadcasted_iota(jnp.int32, (tokens, items), 1)
    hit0 = table == first * cap + slot0.astype(jnp.int32)
    hit1 = table == second * cap + slot1.astype(jnp.int32)
    comb = jnp.where(hit0, weights_ref[:, 0:1], 0.0) + jnp.where(hit1, weights_ref[:, 1:2], 0.0)
    comb_hi = comb.astype(bf16)
    comb_hi_ref[...] = comb_hi
    comb_lo_ref[...] = (comb - comb_hi.astype(f32)).astype(bf16)
    onehot = (jnp.where(hit0, 1.0, 0.0) + jnp.where(hit1, 1.0, 0.0)).astype(bf16)
    lanes = sel_ref.shape[1]
    eye_row = lax.broadcasted_iota(jnp.int32, (tokens, lanes), 0)
    eye_col = lax.broadcasted_iota(jnp.int32, (tokens, lanes), 1)
    eye = jnp.where(eye_row == eye_col, 1.0, 0.0).astype(bf16)
    sel_ref[...] = lax.dot_general(
        onehot, eye, (((0,), (0,)), ((), ())), preferred_element_type=f32
    ).astype(bf16)

    def rounded_rows(weight):
        return matmul(normed, weight[...]).astype(bf16).astype(f32)

    loads[0].wait()
    drive = matmul(normed, fw[...])
    log_sig = jnp.minimum(drive, 0.0) - jnp.log1p(jnp.exp(-jnp.abs(drive)))
    decay[...] = jnp.exp(log_sig / TAU_DECAY + shift_ref[...]).reshape(decay.shape)
    loads[1].wait()
    key[...] = rounded_rows(kw).reshape(key.shape)
    loads[2].wait()
    query[...] = (rounded_rows(qw) * key_dim ** (-0.5)).reshape(query.shape)
    loads[3].wait()
    value[...] = rounded_rows(vw).reshape(value.shape)

    @pl.loop(0, groups)
    def _(g):
        fetch(g).wait()
        for h in range(heads):
            keys = slice(h * key_dim, (h + 1) * key_dim)
            vals = slice(h * value_dim, (h + 1) * value_dim)
            decay_cols = jnp.transpose(decay[g, :, keys])
            key_cols = jnp.transpose(key[g, :, keys])
            query_cols = jnp.transpose(query[g, :, keys])
            for j in range(8):
                fresh = (
                    decay_cols[:, j : j + 1] * state[g * 8 + j, h]
                    + key_cols[:, j : j + 1] * value[g, j : j + 1, vals]
                )
                state[g * 8 + j, h] = fresh
                readout[g, j : j + 1, vals] = jnp.sum(
                    query_cols[:, j : j + 1] * fresh, axis=0, keepdims=True
                )
        put(g).start()

    loads[4].wait()
    outgate = rounded_rows(ow)
    out = readout[...].reshape(tokens, heads * value_dim)
    for h in range(heads):
        vals = slice(h * value_dim, (h + 1) * value_dim)
        part = out[:, vals]
        gain = head_gain_ref[:, vals].astype(f32)
        gated_ref[:, vals] = (part * rms_factor(part) * gain * silu(outgate[:, vals])).astype(bf16)
    for g in range(groups):
        put(g).wait()


def run_attention(hidden, gain, shift, head_gain, routes, weights, qw, kw, vw, ow, fw, state, n_ep):
    bf16, f32 = jnp.bfloat16, jnp.float32
    tokens, heads, key_dim, value_dim = state.shape
    capacity = tokens * routes.shape[1] // n_ep + 2
    cap = (capacity + 15) // 16 * 16
    items = n_ep * cap
    groups = tokens // 8
    lanes = (tokens + 127) // 128 * 128
    vmem = pl.BlockSpec(memory_space=pltpu.VMEM)
    anyspace = pl.BlockSpec(memory_space=pl.ANY)
    gated, sel, comb_hi, comb_lo, new_state = pl.pallas_call(
        functools.partial(attention_kernel, cap),
        out_shape=(
            jax.ShapeDtypeStruct((tokens, heads * value_dim), bf16),
            jax.ShapeDtypeStruct((items, lanes), bf16),
            jax.ShapeDtypeStruct((tokens, items), bf16),
            jax.ShapeDtypeStruct((tokens, items), bf16),
            jax.ShapeDtypeStruct(state.shape, f32),
        ),
        in_specs=[vmem] * 6 + [anyspace] * 6,
        out_specs=(vmem, vmem, vmem, vmem, anyspace),
        scratch_shapes=[pltpu.VMEM(w.shape, bf16) for w in (qw, kw, vw, ow, fw)]
        + [
            pltpu.VMEM(state.shape, f32),
            pltpu.VMEM((groups, 8, heads * key_dim), f32),
            pltpu.VMEM((groups, 8, heads * key_dim), f32),
            pltpu.VMEM((groups, 8, heads * value_dim), f32),
            pltpu.VMEM((groups, 8, heads * key_dim), f32),
            pltpu.VMEM((groups, 8, heads * value_dim), f32),
            pltpu.SemaphoreType.DMA((5,)),
            pltpu.SemaphoreType.DMA((groups,)),
            pltpu.SemaphoreType.DMA((groups,)),
        ],
        compiler_params=pltpu.CompilerParams(vmem_limit_bytes=60 * 1024 * 1024),
    )(hidden, gain, shift, head_gain, routes, weights, qw, kw, vw, ow, fw, state)
    return gated, sel.reshape(n_ep, cap, lanes), comb_hi, comb_lo, new_state


def body(
    hidden_in,
    carried_state,
    input_gain,
    query_weight,
    key_weight,
    value_weight,
    outgate_weight,
    decay_weight,
    decay_shift,
    head_gain,
    output_weight,
    channel_gain,
    branch_gate,
    routes,
    route_weights,
    expert_gate,
    expert_up,
    expert_down,
    dense_gate,
    dense_up,
    dense_down,
):
    gated, sel, comb_hi, comb_lo, new_state = run_attention(
        hidden_in,
        input_gain[None, :],
        decay_shift,
        head_gain.reshape(1, -1),
        routes,
        route_weights,
        query_weight,
        key_weight,
        value_weight,
        outgate_weight,
        decay_weight,
        carried_state,
        lax.axis_size("ep"),
    )
    mixed = run_layer(
        gated,
        output_weight,
        hidden_in,
        channel_gain[None, :],
        branch_gate[None, :],
        sel,
        comb_hi,
        comb_lo,
        expert_gate[0],
        expert_up[0],
        expert_down[0],
        dense_gate,
        dense_up,
        dense_down,
    )
    return (mixed, new_state)


def solution(mesh):
    in_specs = (
        P("ep", None),
        P("ep", "tp", None, None),
        P(),
        P(None, "tp"),
        P(None, "tp"),
        P(None, "tp"),
        P(None, "tp"),
        P(None, "tp"),
        P("ep", "tp"),
        P("tp", None),
        P("tp", None),
        P(),
        P(),
        P("ep", None),
        P("ep", None),
        P("ep", None, "tp"),
        P("ep", None, "tp"),
        P("ep", "tp", None),
        P("tp", "ep"),
        P("tp", "ep"),
        P("ep", "tp"),
    )
    out_specs = (P("ep", "tp"), P("ep", "tp", None, None))
    return jax.shard_map(body, mesh=mesh, in_specs=in_specs, out_specs=out_specs, check_vma=False)
```

profile of v0, /device:TPU:0, one launch (start us, length us, event | category | flops | bytes accessed | tf_op | source)
XLA Modules:
  0.0 72.5 jit_solution(13574116025593254772)
XLA Ops:
  0.6 1.4 %copy.23.routes_ref = s32[48,2]{1,0:T(8,128)} copy(s32[48,2]{0,1:T(2,128)} %param.34) | data formatting | bytes 768 | tf_op args[13]
  2.0 1.4 %copy.24.weights_ref = f32[48,2]{1,0:T(8,128)} copy(f32[48,2]{0,1:T(2,128)} %param.35) | data formatting | bytes 768 | tf_op args[14]
  3.4 1.3 %broadcast_in_dim.9.gain_ref = bf16[1,2048]{1,0:T(2,128)(2,1)} reshape(bf16[2048]{0:T(1024)(128)(2,1)} %param.23) | data formatting | bytes 8192 | tf_op jit(solution)/shard_map/broadcast_in_dim | solution.py:535
  4.7 0.0 copy-start
  4.7 0.0 copy-start.1
  4.7 9.9 %shard_map.212 = (bf16[48,256]{1,0:T(8,128)(2,1)}, bf16[128,128]{1,0:T(8,128)(2,1)}, bf16[48,128]{1,0:T(8,128)(2,1)}, bf16[48,128]{1,0:T(8,128)(2,1)}, f32[48,1,128,256]{3,2,1,0:T(8,128)}) custom-call(bf16[48,2048]{1,0:T(8,128)(2,1)} %hid_ref.1, bf16[1,2048]{1,0:T(2,128)(2,1)} %broadcast_in_dim.9.gain_ref, f32[48,128]{1,0:T(8,128)} %shift_ref.1, ...), custom_call_target="tpu_custom_call" | custom-call | tf_op jit(solution)/shard_map/pallas_call | solution.py:482
  14.5 0.0 copy-done
  14.6 0.6 broadcast_in_dim.10.gain_ref
  15.2 0.0 copy-done.1
  15.2 0.6 broadcast_in_dim.11.gate_ref
  15.8 55.3 %shard_map.213 = bf16[48,512]{1,0:T(8,128)(2,1)} custom-call(bf16[48,256]{1,0:T(8,128)(2,1)} %get-tuple-element.7.gated_ref, bf16[256,2048]{1,0:T(8,128)(2,1)} %outw_ref.1, bf16[48,2048]{1,0:T(8,128)(2,1)} %hid_ref.1, bf16[1,2048]{1,0:T(2,128)(2,1)} %broadcast_in_dim.10.gain_ref, bf16[1,2048]{1,0:T(2,128)(2,1)} %broadcast_in_dim.11.gate_ref, ...), custom_call_target="tpu_custom_call" | custom-call | tf_op jit(solution)/shard_map/pallas_call | solution.py:328
  71.1 1.4 %copy.26 = bf16[48,512]{1,0:T(8,128)(2,1)} copy(bf16[48,512]{1,0:T(8,128)(2,1)} %shard_map.213) | data formatting | bytes 98304
Async XLA Ops:
  4.7 9.9 %copy-start = (bf16[2048]{0:T(1024)(128)(2,1)S(1)}, bf16[2048]{0:T(1024)(128)(2,1)}, u32[]{:S(2)}) copy-start(bf16[2048]{0:T(1024)(128)(2,1)} %param.32) | copy-start | bytes 12292
  4.7 10.5 %copy-start.1 = (bf16[2048]{0:T(1024)(128)(2,1)S(1)}, bf16[2048]{0:T(1024)(128)(2,1)}, u32[]{:S(2)}) copy-start(bf16[2048]{0:T(1024)(128)(2,1)} %param.33) | copy-start | bytes 12292
where the time goes:
time: 72.8 us; the launch traced here: 72.5 us
  Pallas kernels  65.2 us (90%)
  local copies, waits for them, and re-layouts  6.65 us (9%)
    pallas_call x1, Pallas kernels, run_layer(): pl.pallas_call(functools.partial(layer_kernel, n_ep, n_tp), out_shape=jax...  55.3 us
    pallas_call x1, Pallas kernels, run_attention(): pl.pallas_call(functools.partial(attention_kernel, cap), out_shape=(jax.S...  9.88 us
    unnamed x7, local copies, waits for them, and re-layouts  4.17 us

commit v1 on v0

--- a/solution.py
+++ b/solution.py
@@ -18,6 +18,11 @@
 
 def matmul(left, right):
     return jnp.dot(left, right, preferred_element_type=jnp.float32)
+
+
+def flat_row(ref):
+    rows = ref[...].astype(jnp.float32)
+    return jnp.concatenate([rows[k : k + 1, :] for k in range(rows.shape[0])], axis=1)
 
 
 def silu(values):
@@ -74,6 +79,8 @@
     tp_rsem,
     ep_ssem,
     ep_rsem,
+    gain_row,
+    gate_row,
 ):
     f32, bf16 = jnp.float32, jnp.bfloat16
     ep = lax.axis_index("ep")
@@ -91,6 +98,8 @@
         load.start()
         loads.append(load)
 
+    gain_row[...] = flat_row(gain_ref)
+    gate_row[...] = flat_row(gate_ref)
     barrier = pltpu.get_barrier_semaphore()
     for d in range(1, n_tp):
         pl.semaphore_signal(
@@ -182,9 +191,9 @@
         c_part[d - 1].wait_recv()
         attended = attended + p_recv[d - 1].astype(f32)
     middle = (hid_ref[:, own].astype(f32) + attended).astype(bf16).astype(f32)
-    gain = gain_ref[:, own].astype(f32)
+    gain = gain_row[:, own]
     squares = jnp.sum(middle * middle, axis=-1, keepdims=True)
-    inner = jnp.sum(middle * gain * gate_ref[:, own].astype(f32), axis=-1, keepdims=True)
+    inner = jnp.sum(middle * gain * gate_row[:, own], axis=-1, keepdims=True)
     lane = lax.broadcasted_iota(jnp.int32, (tokens, 128), 1)
     st_send[...] = jnp.where(lane < 64, squares, inner)
     c_stat = over_tp(1, lambda peer: st_send, lambda d: st_recv.at[d - 1])
@@ -277,7 +286,10 @@
         dense = dense + out_recv[d - 1].astype(f32)
     arrive(c_ret)
     answers = ret[...].reshape(n_ep * cap, quarter)
-    routed = matmul(comb_hi_ref[...], answers) + matmul(comb_lo_ref[...], answers)
+    over_items = (((0,), (0,)), ((), ()))
+    routed = lax.dot_general(
+        comb_hi_ref[...], answers, over_items, preferred_element_type=f32
+    ) + lax.dot_general(comb_lo_ref[...], answers, over_items, preferred_element_type=f32)
     mixed_ref[...] = (mid_buf[...] + br_buf[:, 0:1] * dense + routed).astype(bf16)
 
     for copies in (c_part, c_sel, c_stat, c_g, c_u, c_eo, c_out, c_ret, *sent):
@@ -324,6 +336,8 @@
         pltpu.SemaphoreType.DMA((7, n_tp - 1)),
         pltpu.SemaphoreType.DMA((4, n_ep - 1)),
         pltpu.SemaphoreType.DMA((4, n_ep - 1)),
+        pltpu.VMEM((1, hid.shape[1]), f32),
+        pltpu.VMEM((1, hid.shape[1]), f32),
     ]
     return pl.pallas_call(
         functools.partial(layer_kernel, n_ep, n_tp),
@@ -394,34 +408,29 @@
         fetch(g).start()
 
     inputs = hidden_ref[...].astype(f32)
-    normed = (inputs * rms_factor(inputs) * gain_ref[...].astype(f32)).astype(bf16)
-
-    items = comb_hi_ref.shape[1]
-    lane = lax.broadcasted_iota(jnp.int32, (tokens, 128), 1)
-    first, second = routes_ref[:, 0:1], routes_ref[:, 1:2]
-    chosen0 = jnp.where(lane == first, 1.0, 0.0)
-    chosen1 = jnp.where(lane == second, 1.0, 0.0)
+    normed = (inputs * rms_factor(inputs) * flat_row(gain_ref)).astype(bf16)
+
+    items = comb_hi_ref.shape[0]
+    experts = (items // cap + 7) // 8 * 8
+    first, second = routes_ref[0:1, :], routes_ref[1:2, :]
+    expert = lax.broadcasted_iota(jnp.int32, (experts, tokens), 0)
+    chosen0 = jnp.where(expert == first, 1.0, 0.0)
+    chosen1 = jnp.where(expert == second, 1.0, 0.0)
     row = lax.broadcasted_iota(jnp.int32, (tokens, tokens), 0)
     col = lax.broadcasted_iota(jnp.int32, (tokens, tokens), 1)
-    before = jnp.where(row > col, 1.0, 0.0).astype(bf16)
-    earlier = matmul(before, (chosen0 + chosen1).astype(bf16))
-    slot0 = jnp.sum(earlier * chosen0, axis=1, keepdims=True)
-    slot1 = jnp.sum(earlier * chosen1, axis=1, keepdims=True)
-    table = lax.broadcasted_iota(jnp.int32, (tokens, items), 1)
+    before = jnp.where(row < col, 1.0, 0.0).astype(bf16)
+    earlier = matmul((chosen0 + chosen1).astype(bf16), before)
+    slot0 = jnp.sum(earlier * chosen0, axis=0, keepdims=True)
+    slot1 = jnp.sum(earlier * chosen1, axis=0, keepdims=True)
+    table = lax.broadcasted_iota(jnp.int32, (items, tokens), 0)
     hit0 = table == first * cap + slot0.astype(jnp.int32)
     hit1 = table == second * cap + slot1.astype(jnp.int32)
-    comb = jnp.where(hit0, weights_ref[:, 0:1], 0.0) + jnp.where(hit1, weights_ref[:, 1:2], 0.0)
+    comb = jnp.where(hit0, weights_ref[0:1, :], 0.0) + jnp.where(hit1, weights_ref[1:2, :], 0.0)
     comb_hi = comb.astype(bf16)
     comb_hi_ref[...] = comb_hi
     comb_lo_ref[...] = (comb - comb_hi.astype(f32)).astype(bf16)
-    onehot = (jnp.where(hit0, 1.0, 0.0) + jnp.where(hit1, 1.0, 0.0)).astype(bf16)
-    lanes = sel_ref.shape[1]
-    eye_row = lax.broadcasted_iota(jnp.int32, (tokens, lanes), 0)
-    eye_col = lax.broadcasted_iota(jnp.int32, (tokens, lanes), 1)
-    eye = jnp.where(eye_row == eye_col, 1.0, 0.0).astype(bf16)
-    sel_ref[...] = lax.dot_general(
-        onehot, eye, (((0,), (0,)), ((), ())), preferred_element_type=f32
-    ).astype(bf16)
+    sel_ref[...] = jnp.zeros(sel_ref.shape, bf16)
+    sel_ref[:, :tokens] = (jnp.where(hit0, 1.0, 0.0) + jnp.where(hit1, 1.0, 0.0)).astype(bf16)
 
     def rounded_rows(weight):
         return matmul(normed, weight[...]).astype(bf16).astype(f32)
@@ -472,7 +481,7 @@
 def run_attention(hidden, gain, shift, head_gain, routes, weights, qw, kw, vw, ow, fw, state, n_ep):
     bf16, f32 = jnp.bfloat16, jnp.float32
     tokens, heads, key_dim, value_dim = state.shape
-    capacity = tokens * routes.shape[1] // n_ep + 2
+    capacity = tokens * routes.shape[0] // n_ep + 2
     cap = (capacity + 15) // 16 * 16
     items = n_ep * cap
     groups = tokens // 8
@@ -484,8 +493,8 @@
         out_shape=(
             jax.ShapeDtypeStruct((tokens, heads * value_dim), bf16),
             jax.ShapeDtypeStruct((items, lanes), bf16),
-            jax.ShapeDtypeStruct((tokens, items), bf16),
-            jax.ShapeDtypeStruct((tokens, items), bf16),
+            jax.ShapeDtypeStruct((items, tokens), bf16),
+            jax.ShapeDtypeStruct((items, tokens), bf16),
             jax.ShapeDtypeStruct(state.shape, f32),
         ),
         in_specs=[vmem] * 6 + [anyspace] * 6,
@@ -532,11 +541,11 @@
 ):
     gated, sel, comb_hi, comb_lo, new_state = run_attention(
         hidden_in,
-        input_gain[None, :],
+        input_gain.reshape(-1, 128),
         decay_shift,
         head_gain.reshape(1, -1),
-        routes,
-        route_weights,
+        routes.T,
+        route_weights.T,
         query_weight,
         key_weight,
         value_weight,
@@ -549,8 +558,8 @@
         gated,
         output_weight,
         hidden_in,
-        channel_gain[None, :],
-        branch_gate[None, :],
+        channel_gain.reshape(-1, 128),
+        branch_gate.reshape(-1, 128),
         sel,
         comb_hi,
         comb_lo,

time: 72.8 us -> 67.6 us (0.929)
  local copies, waits for them, and re-layouts: 6.65 us -> 1.42 us
    unnamed x7 -> x1, local copies, waits for them, and re-layouts: 4.17 us -> 1.42 us
    broadcast_in_dim x3 -> x0, local copies, waits for them, and re-layouts: 2.48 us -> none  [the longest x1 1.28 us: body(): input_gain[None, :]]
where the time goes in v1:
time: 67.6 us; the launch traced here: 67.4 us
  Pallas kernels  65.3 us (97%)
  local copies, waits for them, and re-layouts  1.42 us (2%)
    pallas_call x1, Pallas kernels, run_layer(): pl.pallas_call(functools.partial(layer_kernel, n_ep, n_tp), out_shape=jax...  55.4 us
    pallas_call x1, Pallas kernels, run_attention(): pl.pallas_call(functools.partial(attention_kernel, cap), out_shape=(jax.S...  9.87 us
    unnamed x1, local copies, waits for them, and re-layouts  1.42 us

profile of v1, /device:TPU:0, one launch (start us, length us, event | category | flops | bytes accessed | tf_op | source)
XLA Modules:
  0.0 67.4 jit_solution(13008282292132491874)
XLA Ops:
  0.6 9.9 %shard_map.212 = (bf16[48,256]{1,0:T(8,128)(2,1)}, bf16[128,128]{1,0:T(8,128)(2,1)}, bf16[128,48]{1,0:T(8,128)(2,1)}, bf16[128,48]{1,0:T(8,128)(2,1)}, f32[48,1,128,256]{3,2,1,0:T(8,128)}) custom-call(bf16[48,2048]{1,0:T(8,128)(2,1)} %hid_ref.1, bf16[16,128]{1,0:T(8,128)(2,1)} %bitcast.13, f32[48,128]{1,0:T(8,128)} %shift_ref.1, ...), custom_call_target="tpu_custom_call" | custom-call | tf_op jit(solution)/shard_map/pallas_call | solution.py:491
  10.5 55.4 %shard_map.213 = bf16[48,512]{1,0:T(8,128)(2,1)} custom-call(bf16[48,256]{1,0:T(8,128)(2,1)} %get-tuple-element.7.gated_ref, bf16[256,2048]{1,0:T(8,128)(2,1)} %outw_ref.1, bf16[48,2048]{1,0:T(8,128)(2,1)} %hid_ref.1, bf16[16,128]{1,0:T(8,128)(2,1)} %bitcast.14, bf16[16,128]{1,0:T(8,128)(2,1)} %bitcast.15, bf16[8,16,128]{2,1,0:T(8,128)(2,1)} %bitcast.12, ...), custom_call_target="tpu_custom_call" | custom-call | tf_op jit(solution)/shard_map/pallas_call | solution.py:342
  65.9 1.4 %copy.24 = bf16[48,512]{1,0:T(8,128)(2,1)} copy(bf16[48,512]{1,0:T(8,128)(2,1)} %shard_map.213) | data formatting | bytes 98304

commit v2 on v1

v2 whole, which is shorter than its diff:
```python
import functools

import jax
import jax.numpy as jnp
from jax import lax
from jax.experimental import pallas as pl
from jax.experimental.pallas import tpu as pltpu
from jax.sharding import PartitionSpec as P

EPSILON = 1e-06
TAU_DECAY = 16.0
MESH = pl.DeviceIdType.MESH


def rms_factor(values):
    return lax.rsqrt(jnp.mean(values * values, axis=-1, keepdims=True) + EPSILON)


def matmul(left, right):
    return jnp.dot(left, right, preferred_element_type=jnp.float32)


def flat_row(ref):
    rows = ref[...].astype(jnp.float32)
    return jnp.concatenate([rows[k : k + 1, :] for k in range(rows.shape[0])], axis=1)


def silu(values):
    return values * jax.nn.sigmoid(values)


def layer_kernel(
    n_ep,
    n_tp,
    gated_ref,
    outw_ref,
    hid_ref,
    gain_ref,
    gate_ref,
    sel_ref,
    eg_hbm,
    eu_hbm,
    ed_hbm,
    dg_hbm,
    du_hbm,
    dd_hbm,
    mixed_ref,
    eg,
    eu,
    ed,
    wg,
    wu,
    ddw,
    gain_row,
    gate_row,
    sel_recv,
    p_send,
    p_recv,
    stat,
    scale_rows,
    mid_buf,
    piece,
    other,
    rows_all,
    row_scale,
    gu_send,
    gu_recv,
    gu_own,
    e_hid,
    near_send,
    near_recv,
    far_send,
    far_recv,
    eo_own,
    d_hid,
    d_out,
    y_send,
    y_recv,
    z_send,
    z_recv,
    w_sem,
    ssem,
    rsem,
):
    f32, bf16 = jnp.float32, jnp.bfloat16
    ep = lax.axis_index("ep")
    tp = lax.axis_index("tp")
    tokens, width = hid_ref.shape
    quarter = width // n_tp
    cap, lanes = sel_ref.shape[1:]
    units = dg_hbm.shape[1]
    n_z, half = n_ep // 2, n_tp // 2
    h, c = lax.div(tp, 2), lax.rem(tp, 2)
    partner = tp + 1 - 2 * c
    near = ep + 1 - 2 * lax.rem(ep, 2)
    steps = [0] + sorted(range(1, n_z), key=lambda m: abs(m - n_z // 2))
    own = pl.ds(pl.multiple_of(tp * quarter, quarter), quarter)

    def columns(q):
        return pl.ds(pl.multiple_of(q * quarter, quarter), quarter)

    def member(t, r):
        return lax.rem((near if r else ep) - 2 * steps[t] + n_ep, n_ep)

    def peer(dh, dc):
        return lax.rem(h + dh, half) * 2 + lax.rem(c + dc, 2)

    loads = []
    pairs = ((dg_hbm, wg.at[c]), (du_hbm, wu.at[c]), (eg_hbm, eg), (eu_hbm, eu))
    for i, (src, dst) in enumerate(pairs + ((ed_hbm, ed), (dd_hbm, ddw))):
        load = pltpu.make_async_copy(src, dst, w_sem.at[i])
        load.start()
        loads.append(load)

    gain_row[...] = flat_row(gain_ref)
    gate_row[...] = flat_row(gate_ref)
    barrier = pltpu.get_barrier_semaphore()
    for d in range(1, n_tp):
        pl.semaphore_signal(
            barrier, inc=1, device_id=(ep, lax.rem(tp + d, n_tp)), device_id_type=MESH
        )
    for d in range(1, n_ep):
        pl.semaphore_signal(
            barrier, inc=1, device_id=(lax.rem(ep + d, n_ep), tp), device_id_type=MESH
        )

    sent = []

    def send(src, dst, device):
        copy = pltpu.make_async_remote_copy(
            src_ref=src,
            dst_ref=dst,
            send_sem=ssem.at[len(sent)],
            recv_sem=rsem.at[len(sent)],
            device_id=device,
            device_id_type=MESH,
        )
        copy.start()
        sent.append(copy)
        return copy

    peers = [(dh, dc) for dh in range(1, half) for dc in range(2)] + [(0, 1)]
    for i, (dh, dc) in enumerate(peers):
        part = matmul(gated_ref[...], outw_ref[:, columns(peer(dh, dc))])
        p_send[i] = part.astype(bf16)
    pl.semaphore_wait(barrier, n_tp + n_ep - 2)
    c_part = []
    for i, (dh, dc) in enumerate(peers):
        c_part.append(send(p_send.at[i], p_recv.at[i], (ep, peer(dh, dc))))
    c_sel = []
    for d in range(1, n_ep):
        target = lax.rem(ep + d, n_ep)
        c_sel.append(send(sel_ref.at[target], sel_recv.at[ep], (target, tp)))
    c_dense = [
        send(dg_hbm, wg.at[c], (ep, partner)),
        send(du_hbm, wu.at[c], (ep, partner)),
    ]
    sel_recv[ep] = sel_ref[ep]
    attended = matmul(gated_ref[...], outw_ref[:, own]).astype(bf16).astype(f32)
    for i in reversed(range(len(peers))):
        c_part[i].wait_recv()
        attended = attended + p_recv[i].astype(f32)
    middle = (hid_ref[:, own].astype(f32) + attended).astype(bf16).astype(f32)
    shaped = middle * gain_row[:, own]
    piece[ep] = shaped.astype(bf16)
    squares = jnp.sum(middle * middle, axis=-1, keepdims=True)
    inner = jnp.sum(shaped * gate_row[:, own], axis=-1, keepdims=True)
    line = lax.broadcasted_iota(jnp.int32, (tokens, lanes), 0)
    lane = lax.broadcasted_iota(jnp.int32, (tokens, lanes), 1)
    eye = jnp.where(line == lane, 1.0, 0.0)
    stat[tp, ep, 0:1, :] = jnp.sum(eye * squares, axis=0, keepdims=True)
    stat[tp, ep, 1:2, :] = jnp.sum(eye * inner, axis=0, keepdims=True)
    c_near = send(piece.at[ep], piece.at[ep], (near, tp))
    c_stat = []
    for d in range(1, n_ep):
        target = lax.rem(ep + d, n_ep)
        c_stat.append(send(stat.at[tp, ep], stat.at[tp, ep], (target, tp)))
    c_z = [None]
    for t in range(1, n_z):
        target = lax.rem(ep + 2 * steps[t], n_ep)
        c_z.append(send(piece.at[ep], piece.at[ep], (target, tp)))
    mid_buf[...] = middle

    c_other = {}

    def share(t, r):
        block = member(t, r)
        c_other[t, r] = send(piece.at[block], other.at[block], (ep, partner))

    def pick(q, t, r, source):
        block = member(t, r)
        picked = matmul(sel_recv[block][:, :tokens], source[block]).astype(bf16)
        rows_all[q, (2 * t + r) * cap : (2 * t + r + 1) * cap, :] = picked

    share(0, 0)
    for copy in c_sel:
        copy.wait_recv()
    pick(tp, 0, 0, piece)
    c_near.wait_recv()
    share(0, 1)
    pick(tp, 0, 1, piece)
    c_relay = [None]
    for t in range(1, n_z):
        c_z[t].wait_recv()
        block = member(t, 0)
        c_relay.append(send(piece.at[block], piece.at[block], (near, tp)))
        share(t, 0)
        pick(tp, t, 0, piece)
    for copy in c_stat:
        copy.wait_recv()
    c_total = []
    for dh, dc in peers:
        c_total.append(send(stat.at[tp], stat.at[tp], (ep, peer(dh, dc))))

    groups = n_z // half
    per_part = n_z // 2
    c_rows, c_gu = {}, {}

    def send_rows(part):
        span = pl.ds(2 * part * per_part * cap, 2 * per_part * cap)
        for dh in range(1, half):
            q = peer(dh, 0)
            c_rows[part, dh] = send(rows_all.at[tp, span], rows_all.at[tp, span], (ep, q))

    def partial(j, dh):
        t = j * half + lax.rem(h + dh, half)
        m = steps[j * half]
        for k in range(1, half):
            m = jnp.where(t == j * half + k, steps[j * half + k], m)
        block = lax.rem(jnp.where(c == 1, near, ep) - 2 * m + n_ep, n_ep)
        left, right = piece[block], other[block]
        gate_part = matmul(left, wg[c]) + matmul(right, wg[1 - c])
        up_part = matmul(left, wu[c]) + matmul(right, wu[1 - c])
        return gate_part, up_part, block

    def send_partial(j):
        for dh in range(1, half):
            gate_part, up_part, _ = partial(j, dh)
            gu_send[j, dh - 1, 0] = gate_part.astype(bf16)
            gu_send[j, dh - 1, 1] = up_part.astype(bf16)
            source, target = gu_send.at[j, dh - 1], gu_recv.at[j, dh - 1]
            c_gu[j, dh] = send(source, target, (ep, peer(dh, 0)))

    def wait_other(ts):
        for t in ts:
            for r in range(2):
                c_other[t, r].wait_recv()

    ready = [False]

    def dense_ready():
        if not ready[0]:
            loads[0].wait()
            loads[1].wait()
            for copy in c_dense:
                copy.wait_recv()
            ready[0] = True

    for part in range(2):
        ts = range(part * per_part, (part + 1) * per_part)
        for t in ts:
            if t:
                c_relay[t].wait_recv()
                share(t, 1)
                pick(tp, t, 1, piece)
        send_rows(part)
        dense_ready()
        wait_other(ts)
        for j in range(part * groups // 2, (part + 1) * groups // 2):
            send_partial(j)
    blocks = []
    for j in range(groups):
        gate_part, up_part, block = partial(j, 0)
        gu_own[j, 0] = gate_part
        gu_own[j, 1] = up_part
        blocks.append(block)
    for t in range(n_z):
        for r in range(2):
            pick(partner, t, r, other)
    for copy in c_total:
        copy.wait_recv()
    totals = stat[0]
    for q in range(1, n_tp):
        totals = totals + stat[q]
    factors = lax.rsqrt(totals[:, 0:1, :] / width + EPSILON)
    scale_rows[:, 0:1, :] = factors
    scale_rows[:, 1:2, :] = jax.nn.sigmoid(totals[:, 1:2, :] * factors)
    for t in range(n_z):
        for r in range(2):
            block = member(t, r)
            chosen = sel_recv[block].astype(f32)
            chosen_lane = lax.broadcasted_iota(jnp.int32, (cap, lanes), 1)
            masked = jnp.where(chosen_lane < tokens, chosen * scale_rows[block, 0:1, :], 0.0)
            column = jnp.sum(masked, axis=1, keepdims=True)
            at = slice((2 * t + r) * cap, (2 * t + r + 1) * cap)
            row_scale[at, :] = jnp.broadcast_to(column, (cap, lanes))

    c_pass = []
    for part in range(2):
        span = pl.ds(2 * part * per_part * cap, 2 * per_part * cap)
        for dh in range(1, half):
            c_rows[part, dh].wait_recv()
            q = lax.rem(h - dh + half, half) * 2 + c
            c_pass.append(send(rows_all.at[q, span], rows_all.at[q, span], (ep, partner)))

    def column_of(row):
        return jnp.sum(eye * row, axis=1, keepdims=True)

    for j in range(groups):
        gate_sum, up_sum = gu_own[j, 0], gu_own[j, 1]
        for dh in range(1, half):
            c_gu[j, dh].wait_recv()
            gate_sum = gate_sum + gu_recv[j, dh - 1, 0].astype(f32)
            up_sum = up_sum + gu_recv[j, dh - 1, 1].astype(f32)
        scale = column_of(scale_rows[blocks[j], 0:1, :])
        d_hid[tp, j] = (silu(gate_sum * scale) * (up_sum * scale)).astype(bf16)
    c_hid = [send(d_hid.at[tp], d_hid.at[tp], (ep, peer(dh, 0))) for dh in range(1, half)]
    c_hid_near = [send(d_hid.at[tp], d_hid.at[tp], (ep, partner))]

    loads[2].wait()
    loads[3].wait()
    for copy in c_pass:
        copy.wait_recv()
    block = eg.shape[1]
    tile = 256 if block % 256 == 0 else 128

    @pl.loop(0, block // tile)
    def _(i):
        cols = pl.ds(pl.multiple_of(i * tile, tile), tile)
        gate_part = matmul(rows_all[0], eg[0:quarter, cols])
        up_part = matmul(rows_all[0], eu[0:quarter, cols])
        for q in range(1, n_tp):
            span = slice(q * quarter, (q + 1) * quarter)
            gate_part = gate_part + matmul(rows_all[q], eg[span, cols])
            up_part = up_part + matmul(rows_all[q], eu[span, cols])
        scale = row_scale[:, 0:1]
        e_hid[:, cols] = (silu(gate_part * scale) * (up_part * scale)).astype(bf16)

    loads[4].wait()
    c_near_eo = []
    for i, dh in enumerate(list(range(1, half)) + [0]):
        near_send[i] = matmul(e_hid[...], ed[:, columns(peer(dh, 1))]).astype(bf16)
        c_near_eo.append(send(near_send.at[i], near_recv.at[i], (ep, partner)))
    for dh in range(1, half):
        c_hid[dh - 1].wait_recv()
        q = lax.rem(h - dh + half, half) * 2 + c
        c_hid_near.append(send(d_hid.at[q], d_hid.at[q], (ep, partner)))
    c_far = []
    for i, dh in enumerate(range(1, half)):
        part = matmul(e_hid[...], ed[:, columns(peer(dh, 0))])
        c_near_eo[i].wait_recv()
        far_send[i] = (part + near_recv[i].astype(f32)).astype(bf16)
        c_far.append(send(far_send.at[i], far_recv.at[i], (ep, peer(dh, 0))))
    part = matmul(e_hid[...], ed[:, own])
    c_near_eo[half - 1].wait_recv()
    eo_own[...] = part + near_recv[half - 1].astype(f32)
    loads[5].wait()
    for copy in c_hid_near:
        copy.wait_recv()
    hidden = d_hid[...].reshape(n_ep * tokens, units)
    d_out[...] = matmul(hidden, ddw[...]).reshape(d_out.shape)
    total = eo_own[...]
    for i in range(half - 1):
        c_far[i].wait_recv()
        total = total + far_recv[i].astype(f32)
    eo_own[...] = total

    def outcome(t, r):
        block = member(t, r)
        span = slice((2 * t + r) * cap, (2 * t + r + 1) * cap)
        chosen = sel_recv[block]
        weight = chosen[:, lanes - 2 : lanes - 1].astype(f32)
        weight = weight + chosen[:, lanes - 1 : lanes].astype(f32)
        answers = (eo_own[span, :] * weight).astype(bf16)
        routed = lax.dot_general(
            chosen[:, :tokens], answers, (((0,), (0,)), ((), ())), preferred_element_type=f32
        )
        branch = column_of(scale_rows[block, 1:2, :])
        return branch * d_out[(t % half) * 2 + r, t // half] + routed

    order = list(range(1, n_z)) + [0]
    c_y = {}
    for t in order:
        y_send[t] = outcome(t, 1).astype(bf16)
        c_y[t] = send(y_send.at[t], y_recv.at[t], (near, tp))
    c_out = []
    for t in order:
        mine = outcome(t, 0)
        c_y[t].wait_recv()
        mine = mine + y_recv[t].astype(f32)
        if t:
            z_send[t - 1] = mine.astype(bf16)
            c_out.append(send(z_send.at[t - 1], z_recv.at[t - 1], (member(t, 0), tp)))
    mine = mine + mid_buf[...]
    for t in range(1, n_z):
        c_out[t - 1].wait_recv()
        mine = mine + z_recv[t - 1].astype(f32)
    mixed_ref[...] = mine.astype(bf16)
    for copy in sent:
        copy.wait_send()


def run_layer(gated, output_weight, hid, gain, gate, sel, eg, eu, ed, dg, du, dd):
    n_ep, n_tp = lax.axis_size("ep"), lax.axis_size("tp")
    tokens = hid.shape[0]
    quarter = hid.shape[1] // n_tp
    cap, lanes = sel.shape[1:]
    items = n_ep * cap
    n_z, half = n_ep // 2, n_tp // 2
    groups = n_z // half
    units = dg.shape[1]
    bf16, f32 = jnp.bfloat16, jnp.float32
    vmem = pl.BlockSpec(memory_space=pltpu.VMEM)
    anyspace = pl.BlockSpec(memory_space=pl.ANY)
    copies = 8 * n_ep + 4 * n_tp + 6 * n_z + 16
    scratch = [pltpu.VMEM(w.shape, bf16) for w in (eg, eu, ed)]
    scratch += [
        pltpu.VMEM((2, quarter, units), bf16),
        pltpu.VMEM((2, quarter, units), bf16),
        pltpu.VMEM(dd.shape, bf16),
        pltpu.VMEM((1, hid.shape[1]), f32),
        pltpu.VMEM((1, hid.shape[1]), f32),
        pltpu.VMEM(sel.shape, bf16),
        pltpu.VMEM((n_tp - 1, tokens, quarter), bf16),
        pltpu.VMEM((n_tp - 1, tokens, quarter), bf16),
        pltpu.VMEM((n_tp, n_ep, 2, lanes), f32),
        pltpu.VMEM((n_ep, 2, lanes), f32),
        pltpu.VMEM((tokens, quarter), f32),
        pltpu.VMEM((n_ep, tokens, quarter), bf16),
        pltpu.VMEM((n_ep, tokens, quarter), bf16),
        pltpu.VMEM((n_tp, items, quarter), bf16),
        pltpu.VMEM((items, lanes), f32),
        pltpu.VMEM((groups, half - 1, 2, tokens, units), bf16),
        pltpu.VMEM((groups, half - 1, 2, tokens, units), bf16),
        pltpu.VMEM((groups, 2, tokens, units), f32),
        pltpu.VMEM((items, eg.shape[1]), bf16),
        pltpu.VMEM((half, items, quarter), bf16),
        pltpu.VMEM((half, items, quarter), bf16),
        pltpu.VMEM((half - 1, items, quarter), bf16),
        pltpu.VMEM((half - 1, items, quarter), bf16),
        pltpu.VMEM((items, quarter), f32),
        pltpu.VMEM((n_tp, groups, tokens, units), bf16),
        pltpu.VMEM((n_tp, groups, tokens, quarter), f32),
        pltpu.VMEM((n_z, tokens, quarter), bf16),
        pltpu.VMEM((n_z, tokens, quarter), bf16),
        pltpu.VMEM((n_z - 1, tokens, quarter), bf16),
        pltpu.VMEM((n_z - 1, tokens, quarter), bf16),
        pltpu.SemaphoreType.DMA((6,)),
        pltpu.SemaphoreType.DMA((copies,)),
        pltpu.SemaphoreType.DMA((copies,)),
    ]
    return pl.pallas_call(
        functools.partial(layer_kernel, n_ep, n_tp),
        out_shape=jax.ShapeDtypeStruct((tokens, quarter), bf16),
        in_specs=[vmem] * 6 + [anyspace] * 6,
        out_specs=vmem,
        scratch_shapes=scratch,
        compiler_params=pltpu.CompilerParams(
            collective_id=0, has_side_effects=True, vmem_limit_bytes=60 * 1024 * 1024
        ),
    )(gated, output_weight, hid, gain, gate, sel, eg, eu, ed, dg, du, dd)


def attention_kernel(
    cap,
    hidden_ref,
    gain_ref,
    shift_ref,
    head_gain_ref,
    routes_ref,
    weights_ref,
    qw_hbm,
    kw_hbm,
    vw_hbm,
    ow_hbm,
    fw_hbm,
    state_hbm,
    gated_ref,
    sel_ref,
    new_hbm,
    qw,
    kw,
    vw,
    ow,
    fw,
    state,
    query,
    key,
    value,
    decay,
    readout,
    w_sem,
    in_sem,
    out_sem,
):
    f32, bf16 = jnp.float32, jnp.bfloat16
    tokens = hidden_ref.shape[0]
    heads, key_dim, value_dim = state.shape[1:]
    groups = tokens // 8
    loads = []
    pairs = ((fw_hbm, fw), (kw_hbm, kw), (qw_hbm, qw), (vw_hbm, vw), (ow_hbm, ow))
    for i, (src, dst) in enumerate(pairs):
        load = pltpu.make_async_copy(src, dst, w_sem.at[i])
        load.start()
        loads.append(load)

    def fetch(g):
        rows = pl.ds(g * 8, 8)
        return pltpu.make_async_copy(state_hbm.at[rows], state.at[rows], in_sem.at[g])

    def put(g):
        rows = pl.ds(g * 8, 8)
        return pltpu.make_async_copy(state.at[rows], new_hbm.at[rows], out_sem.at[g])

    for g in range(groups):
        fetch(g).start()

    inputs = hidden_ref[...].astype(f32)
    normed = (inputs * rms_factor(inputs) * flat_row(gain_ref)).astype(bf16)

    items, lanes = sel_ref.shape
    experts = (items // cap + 7) // 8 * 8
    first, second = routes_ref[0:1, :], routes_ref[1:2, :]
    expert = lax.broadcasted_iota(jnp.int32, (experts, tokens), 0)
    chosen0 = jnp.where(expert == first, 1.0, 0.0)
    chosen1 = jnp.where(expert == second, 1.0, 0.0)
    row = lax.broadcasted_iota(jnp.int32, (tokens, tokens), 0)
    col = lax.broadcasted_iota(jnp.int32, (tokens, tokens), 1)
    before = jnp.where(row < col, 1.0, 0.0).astype(bf16)
    earlier = matmul((chosen0 + chosen1).astype(bf16), before)
    slot0 = jnp.sum(earlier * chosen0, axis=0, keepdims=True)
    slot1 = jnp.sum(earlier * chosen1, axis=0, keepdims=True)
    table = lax.broadcasted_iota(jnp.int32, (items, tokens), 0)
    hit0 = table == first * cap + slot0.astype(jnp.int32)
    hit1 = table == second * cap + slot1.astype(jnp.int32)
    comb = jnp.where(hit0, weights_ref[0:1, :], 0.0) + jnp.where(hit1, weights_ref[1:2, :], 0.0)
    weight = jnp.sum(comb, axis=1, keepdims=True)
    weight_hi = weight.astype(bf16).astype(f32)
    lane = lax.broadcasted_iota(jnp.int32, (items, lanes), 1)
    tail = jnp.where(lane == lanes - 2, weight_hi, weight - weight_hi)
    sel_ref[...] = jnp.where(lane < lanes - 2, 0.0, tail).astype(bf16)
    sel_ref[:, :tokens] = (jnp.where(hit0, 1.0, 0.0) + jnp.where(hit1, 1.0, 0.0)).astype(bf16)

    def rounded_rows(weight):
        return matmul(normed, weight[...]).astype(bf16).astype(f32)

    loads[0].wait()
    drive = matmul(normed, fw[...])
    log_sig = jnp.minimum(drive, 0.0) - jnp.log1p(jnp.exp(-jnp.abs(drive)))
    decay[...] = jnp.exp(log_sig / TAU_DECAY + shift_ref[...]).reshape(decay.shape)
    loads[1].wait()
    key[...] = rounded_rows(kw).reshape(key.shape)
    loads[2].wait()
    query[...] = (rounded_rows(qw) * key_dim ** (-0.5)).reshape(query.shape)
    loads[3].wait()
    value[...] = rounded_rows(vw).reshape(value.shape)

    @pl.loop(0, groups)
    def _(g):
        fetch(g).wait()
        for h in range(heads):
            keys = slice(h * key_dim, (h + 1) * key_dim)
            vals = slice(h * value_dim, (h + 1) * value_dim)
            decay_cols = jnp.transpose(decay[g, :, keys])
            key_cols = jnp.transpose(key[g, :, keys])
            query_cols = jnp.transpose(query[g, :, keys])
            for j in range(8):
                fresh = (
                    decay_cols[:, j : j + 1] * state[g * 8 + j, h]
                    + key_cols[:, j : j + 1] * value[g, j : j + 1, vals]
                )
                state[g * 8 + j, h] = fresh
                readout[g, j : j + 1, vals] = jnp.sum(
                    query_cols[:, j : j + 1] * fresh, axis=0, keepdims=True
                )
        put(g).start()

    loads[4].wait()
    outgate = rounded_rows(ow)
    out = readout[...].reshape(tokens, heads * value_dim)
    for h in range(heads):
        vals = slice(h * value_dim, (h + 1) * value_dim)
        part = out[:, vals]
        gain = head_gain_ref[:, vals].astype(f32)
        gated_ref[:, vals] = (part * rms_factor(part) * gain * silu(outgate[:, vals])).astype(bf16)
    for g in range(groups):
        put(g).wait()


def run_attention(hidden, gain, shift, head_gain, routes, weights, qw, kw, vw, ow, fw, state, n_ep):
    bf16, f32 = jnp.bfloat16, jnp.float32
    tokens, heads, key_dim, value_dim = state.shape
    capacity = tokens * routes.shape[0] // n_ep + 2
    cap = (capacity + 15) // 16 * 16
    items = n_ep * cap
    groups = tokens // 8
    lanes = (tokens + 2 + 127) // 128 * 128
    vmem = pl.BlockSpec(memory_space=pltpu.VMEM)
    anyspace = pl.BlockSpec(memory_space=pl.ANY)
    gated, sel, new_state = pl.pallas_call(
        functools.partial(attention_kernel, cap),
        out_shape=(
            jax.ShapeDtypeStruct((tokens, heads * value_dim), bf16),
            jax.ShapeDtypeStruct((items, lanes), bf16),
            jax.ShapeDtypeStruct(state.shape, f32),
        ),
        in_specs=[vmem] * 6 + [anyspace] * 6,
        out_specs=(vmem, vmem, anyspace),
        scratch_shapes=[pltpu.VMEM(w.shape, bf16) for w in (qw, kw, vw, ow, fw)]
        + [
            pltpu.VMEM(state.shape, f32),
            pltpu.VMEM((groups, 8, heads * key_dim), f32),
            pltpu.VMEM((groups, 8, heads * key_dim), f32),
            pltpu.VMEM((groups, 8, heads * value_dim), f32),
            pltpu.VMEM((groups, 8, heads * key_dim), f32),
            pltpu.VMEM((groups, 8, heads * value_dim), f32),
            pltpu.SemaphoreType.DMA((5,)),
            pltpu.SemaphoreType.DMA((groups,)),
            pltpu.SemaphoreType.DMA((groups,)),
        ],
        compiler_params=pltpu.CompilerParams(vmem_limit_bytes=60 * 1024 * 1024),
    )(hidden, gain, shift, head_gain, routes, weights, qw, kw, vw, ow, fw, state)
    return gated, sel.reshape(n_ep, cap, lanes), new_state


def body(
    hidden_in,
    carried_state,
    input_gain,
    query_weight,
    key_weight,
    value_weight,
    outgate_weight,
    decay_weight,
    decay_shift,
    head_gain,
    output_weight,
    channel_gain,
    branch_gate,
    routes,
    route_weights,
    expert_gate,
    expert_up,
    expert_down,
    dense_gate,
    dense_up,
    dense_down,
):
    gated, sel, new_state = run_attention(
        hidden_in,
        input_gain.reshape(-1, 128),
        decay_shift,
        head_gain.reshape(1, -1),
        routes.T,
        route_weights.T,
        query_weight,
        key_weight,
        value_weight,
        outgate_weight,
        decay_weight,
        carried_state,
        lax.axis_size("ep"),
    )
    mixed = run_layer(
        gated,
        output_weight,
        hidden_in,
        channel_gain.reshape(-1, 128),
        branch_gate.reshape(-1, 128),
        sel,
        expert_gate[0],
        expert_up[0],
        expert_down[0],
        dense_gate,
        dense_up,
        dense_down,
    )
    return (mixed, new_state)


def solution(mesh):
    in_specs = (
        P("ep", None),
        P("ep", "tp", None, None),
        P(),
        P(None, "tp"),
        P(None, "tp"),
        P(None, "tp"),
        P(None, "tp"),
        P(None, "tp"),
        P("ep", "tp"),
        P("tp", None),
        P("tp", None),
        P(),
        P(),
        P("ep", None),
        P("ep", None),
        P("ep", None, "tp"),
        P("ep", None, "tp"),
        P("ep", "tp", None),
        P("tp", "ep"),
        P("tp", "ep"),
        P("ep", "tp"),
    )
    out_specs = (P("ep", "tp"), P("ep", "tp", None, None))
    return jax.shard_map(body, mesh=mesh, in_specs=in_specs, out_specs=out_specs, check_vma=False)
```

time: 67.6 us -> 60.1 us (0.89)
  Pallas kernels: 65.3 us -> 57.8 us
    pallas_call x1, Pallas kernels: 55.4 us -> 47.9 us  [run_layer(): pl.pallas_call(functools.partial(layer_kernel, n_ep, n_tp), out_shape=jax...]
where the time goes in v2:
time: 60.1 us; the launch traced here: 59.8 us
  Pallas kernels  57.8 us (96%)
  local copies, waits for them, and re-layouts  1.42 us (2%)
  between operations  0.65 us (1%)
    pallas_call x1, Pallas kernels, run_layer(): pl.pallas_call(functools.partial(layer_kernel, n_ep, n_tp), out_shape=jax...  47.9 us
    pallas_call x1, Pallas kernels, run_attention(): pl.pallas_call(functools.partial(attention_kernel, cap), out_shape=(jax.S...  9.84 us
    unnamed x1, local copies, waits for them, and re-layouts  1.42 us

profile of v2, /device:TPU:0, one launch (start us, length us, event | category | flops | bytes accessed | tf_op | source)
XLA Modules:
  0.0 59.8 jit_solution(6801499543193791931)
XLA Ops:
  0.6 9.8 %shard_map.212 = (bf16[48,256]{1,0:T(8,128)(2,1)}, bf16[128,128]{1,0:T(8,128)(2,1)}, f32[48,1,128,256]{3,2,1,0:T(8,128)}) custom-call(bf16[48,2048]{1,0:T(8,128)(2,1)} %hid_ref.1, bf16[16,128]{1,0:T(8,128)(2,1)} %bitcast.13, f32[48,128]{1,0:T(8,128)} %shift_ref.1, bf16[1,256]{1,0:T(2,128)(2,1)} %head_gain_ref.1, s32[2,48]{1,0:T(2,128)} %bitcast.16, ...), custom_call_target="tpu_custom_call" | custom-call | tf_op jit(solution)/shard_map/pallas_call | solution.py:600
  10.5 47.9 %shard_map.213 = bf16[48,512]{1,0:T(8,128)(2,1)} custom-call(bf16[48,256]{1,0:T(8,128)(2,1)} %get-tuple-element.5.gated_ref, bf16[256,2048]{1,0:T(8,128)(2,1)} %outw_ref.1, bf16[48,2048]{1,0:T(8,128)(2,1)} %hid_ref.1, bf16[16,128]{1,0:T(8,128)(2,1)} %bitcast.14, bf16[16,128]{1,0:T(8,128)(2,1)} %bitcast.15, bf16[8,16,128]{2,1,0:T(8,128)(2,1)} %bitcast.12, ...), custom_call_target="tpu_custom_call" | custom-call | tf_op jit(solution)/shard_map/pallas_call | solution.py:452
  58.4 1.4 %copy.24 = bf16[48,512]{1,0:T(8,128)(2,1)} copy(bf16[48,512]{1,0:T(8,128)(2,1)} %shard_map.213) | data formatting | bytes 98304

commit v3 on v2

--- a/solution.py
+++ b/solution.py
@@ -192,178 +192,149 @@
         picked = matmul(sel_recv[block][:, :tokens], source[block]).astype(bf16)
         rows_all[q, (2 * t + r) * cap : (2 * t + r + 1) * cap, :] = picked
 
-    share(0, 0)
-    for copy in c_sel:
-        copy.wait_recv()
-    pick(tp, 0, 0, piece)
-    c_near.wait_recv()
-    share(0, 1)
-    pick(tp, 0, 1, piece)
-    c_relay = [None]
-    for t in range(1, n_z):
-        c_z[t].wait_recv()
-        block = member(t, 0)
-        c_relay.append(send(piece.at[block], piece.at[block], (near, tp)))
-        share(t, 0)
-        pick(tp, t, 0, piece)
-    for copy in c_stat:
-        copy.wait_recv()
-    c_total = []
-    for dh, dc in peers:
-        c_total.append(send(stat.at[tp], stat.at[tp], (ep, peer(dh, dc))))
-
-    groups = n_z // half
+    c_rows, c_pass, c_gu, c_hid, c_hid_near = {}, {}, {}, {}, {}
+    c_eo_near, c_eo_far, c_y, c_out = {}, {}, {}, {}
+    sub = tokens // half
     per_part = n_z // 2
-    c_rows, c_gu = {}, {}
-
-    def send_rows(part):
-        span = pl.ds(2 * part * per_part * cap, 2 * per_part * cap)
+    parts = [range(p * per_part, (p + 1) * per_part) for p in range(2)]
+
+    def of_chip(value, index):
+        chosen = value[:sub]
+        for k in range(1, half):
+            chosen = jnp.where(index == k, value[k * sub : (k + 1) * sub], chosen)
+        return chosen
+
+    def span_of(t):
+        return pl.ds(2 * t * cap, 2 * cap)
+
+    def send_rows(t):
         for dh in range(1, half):
-            q = peer(dh, 0)
-            c_rows[part, dh] = send(rows_all.at[tp, span], rows_all.at[tp, span], (ep, q))
-
-    def partial(j, dh):
-        t = j * half + lax.rem(h + dh, half)
-        m = steps[j * half]
-        for k in range(1, half):
-            m = jnp.where(t == j * half + k, steps[j * half + k], m)
-        block = lax.rem(jnp.where(c == 1, near, ep) - 2 * m + n_ep, n_ep)
+            rows = rows_all.at[tp, span_of(t)]
+            c_rows[t, dh] = send(rows, rows, (ep, peer(dh, 0)))
+
+    def pass_rows(t):
+        for dh in range(1, half):
+            c_rows[t, dh].wait_recv()
+            q = lax.rem(h - dh + half, half) * 2 + c
+            rows = rows_all.at[q, span_of(t)]
+            c_pass[t, dh] = send(rows, rows, (ep, partner))
+
+    def partial(t):
+        for r in range(2):
+            c_other[t, r].wait_recv()
+        block = lax.rem(jnp.where(c == 1, near, ep) - 2 * steps[t] + n_ep, n_ep)
         left, right = piece[block], other[block]
-        gate_part = matmul(left, wg[c]) + matmul(right, wg[1 - c])
-        up_part = matmul(left, wu[c]) + matmul(right, wu[1 - c])
-        return gate_part, up_part, block
-
-    def send_partial(j):
+        for i, w in enumerate((wg, wu)):
+            product = matmul(left, w[c]) + matmul(right, w[1 - c])
+            gu_own[t, i] = of_chip(product, h)
+            for dh in range(1, half):
+                gu_send[t, dh - 1, i] = of_chip(product, lax.rem(h + dh, half)).astype(bf16)
         for dh in range(1, half):
-            gate_part, up_part, _ = partial(j, dh)
-            gu_send[j, dh - 1, 0] = gate_part.astype(bf16)
-            gu_send[j, dh - 1, 1] = up_part.astype(bf16)
-            source, target = gu_send.at[j, dh - 1], gu_recv.at[j, dh - 1]
-            c_gu[j, dh] = send(source, target, (ep, peer(dh, 0)))
-
-    def wait_other(ts):
-        for t in ts:
+            source, target = gu_send.at[t, dh - 1], gu_recv.at[t, dh - 1]
+            c_gu[t, dh] = send(source, target, (ep, peer(dh, 0)))
+
+    line_own = lax.broadcasted_iota(jnp.int32, (sub, lanes), 0) + h * sub
+    eye_own = jnp.where(line_own == lax.broadcasted_iota(jnp.int32, (sub, lanes), 1), 1.0, 0.0)
+
+    def activate(p):
+        shares = []
+        for t in parts[p]:
+            gate_sum, up_sum = gu_own[t, 0], gu_own[t, 1]
+            for dh in range(1, half):
+                c_gu[t, dh].wait_recv()
+                gate_sum = gate_sum + gu_recv[t, dh - 1, 0].astype(f32)
+                up_sum = up_sum + gu_recv[t, dh - 1, 1].astype(f32)
+            block = lax.rem(jnp.where(c == 1, near, ep) - 2 * steps[t] + n_ep, n_ep)
+            scale = jnp.sum(eye_own * scale_rows[block, 0:1, :], axis=1, keepdims=True)
+            shares.append(silu(gate_sum * scale) * (up_sum * scale))
+        d_hid[tp, p] = jnp.concatenate(shares, axis=0).astype(bf16)
+        mine = d_hid.at[tp, p]
+        for dh in range(1, half):
+            c_hid[p, dh] = send(mine, mine, (ep, peer(dh, 0)))
+        c_hid_near[p, 0] = send(mine, mine, (ep, partner))
+
+    def pass_hidden(p):
+        for dh in range(1, half):
+            c_hid[p, dh].wait_recv()
+            got = d_hid.at[lax.rem(h - dh + half, half) * 2 + c, p]
+            c_hid_near[p, dh] = send(got, got, (ep, partner))
+
+    def dense_down(p):
+        for dh in range(half):
+            c_hid_near[p, dh].wait_recv()
+        hidden = d_hid[:, p].reshape(n_tp * per_part * sub, units)
+        d_out[p] = matmul(hidden, ddw[...]).reshape(d_out.shape[1:])
+
+    def scales():
+        for copy in c_total:
+            copy.wait_recv()
+        totals = stat[0]
+        for q in range(1, n_tp):
+            totals = totals + stat[q]
+        factors = lax.rsqrt(totals[:, 0:1, :] / width + EPSILON)
+        scale_rows[:, 0:1, :] = factors
+        scale_rows[:, 1:2, :] = jax.nn.sigmoid(totals[:, 1:2, :] * factors)
+
+    count = 2 * per_part * cap
+    chosen_lane = lax.broadcasted_iota(jnp.int32, (cap, lanes), 1)
+
+    def prepare(p):
+        for t in parts[p]:
             for r in range(2):
-                c_other[t, r].wait_recv()
-
-    ready = [False]
-
-    def dense_ready():
-        if not ready[0]:
-            loads[0].wait()
-            loads[1].wait()
-            for copy in c_dense:
-                copy.wait_recv()
-            ready[0] = True
-
-    for part in range(2):
-        ts = range(part * per_part, (part + 1) * per_part)
-        for t in ts:
-            if t:
-                c_relay[t].wait_recv()
-                share(t, 1)
-                pick(tp, t, 1, piece)
-        send_rows(part)
-        dense_ready()
-        wait_other(ts)
-        for j in range(part * groups // 2, (part + 1) * groups // 2):
-            send_partial(j)
-    blocks = []
-    for j in range(groups):
-        gate_part, up_part, block = partial(j, 0)
-        gu_own[j, 0] = gate_part
-        gu_own[j, 1] = up_part
-        blocks.append(block)
-    for t in range(n_z):
-        for r in range(2):
-            pick(partner, t, r, other)
-    for copy in c_total:
-        copy.wait_recv()
-    totals = stat[0]
-    for q in range(1, n_tp):
-        totals = totals + stat[q]
-    factors = lax.rsqrt(totals[:, 0:1, :] / width + EPSILON)
-    scale_rows[:, 0:1, :] = factors
-    scale_rows[:, 1:2, :] = jax.nn.sigmoid(totals[:, 1:2, :] * factors)
-    for t in range(n_z):
-        for r in range(2):
-            block = member(t, r)
-            chosen = sel_recv[block].astype(f32)
-            chosen_lane = lax.broadcasted_iota(jnp.int32, (cap, lanes), 1)
-            masked = jnp.where(chosen_lane < tokens, chosen * scale_rows[block, 0:1, :], 0.0)
-            column = jnp.sum(masked, axis=1, keepdims=True)
-            at = slice((2 * t + r) * cap, (2 * t + r + 1) * cap)
-            row_scale[at, :] = jnp.broadcast_to(column, (cap, lanes))
-
-    c_pass = []
-    for part in range(2):
-        span = pl.ds(2 * part * per_part * cap, 2 * per_part * cap)
-        for dh in range(1, half):
-            c_rows[part, dh].wait_recv()
-            q = lax.rem(h - dh + half, half) * 2 + c
-            c_pass.append(send(rows_all.at[q, span], rows_all.at[q, span], (ep, partner)))
-
-    def column_of(row):
-        return jnp.sum(eye * row, axis=1, keepdims=True)
-
-    for j in range(groups):
-        gate_sum, up_sum = gu_own[j, 0], gu_own[j, 1]
-        for dh in range(1, half):
-            c_gu[j, dh].wait_recv()
-            gate_sum = gate_sum + gu_recv[j, dh - 1, 0].astype(f32)
-            up_sum = up_sum + gu_recv[j, dh - 1, 1].astype(f32)
-        scale = column_of(scale_rows[blocks[j], 0:1, :])
-        d_hid[tp, j] = (silu(gate_sum * scale) * (up_sum * scale)).astype(bf16)
-    c_hid = [send(d_hid.at[tp], d_hid.at[tp], (ep, peer(dh, 0))) for dh in range(1, half)]
-    c_hid_near = [send(d_hid.at[tp], d_hid.at[tp], (ep, partner))]
-
-    loads[2].wait()
-    loads[3].wait()
-    for copy in c_pass:
-        copy.wait_recv()
-    block = eg.shape[1]
-    tile = 256 if block % 256 == 0 else 128
-
-    @pl.loop(0, block // tile)
-    def _(i):
-        cols = pl.ds(pl.multiple_of(i * tile, tile), tile)
-        gate_part = matmul(rows_all[0], eg[0:quarter, cols])
-        up_part = matmul(rows_all[0], eu[0:quarter, cols])
-        for q in range(1, n_tp):
-            span = slice(q * quarter, (q + 1) * quarter)
-            gate_part = gate_part + matmul(rows_all[q], eg[span, cols])
-            up_part = up_part + matmul(rows_all[q], eu[span, cols])
-        scale = row_scale[:, 0:1]
-        e_hid[:, cols] = (silu(gate_part * scale) * (up_part * scale)).astype(bf16)
-
-    loads[4].wait()
-    c_near_eo = []
-    for i, dh in enumerate(list(range(1, half)) + [0]):
-        near_send[i] = matmul(e_hid[...], ed[:, columns(peer(dh, 1))]).astype(bf16)
-        c_near_eo.append(send(near_send.at[i], near_recv.at[i], (ep, partner)))
-    for dh in range(1, half):
-        c_hid[dh - 1].wait_recv()
-        q = lax.rem(h - dh + half, half) * 2 + c
-        c_hid_near.append(send(d_hid.at[q], d_hid.at[q], (ep, partner)))
-    c_far = []
-    for i, dh in enumerate(range(1, half)):
-        part = matmul(e_hid[...], ed[:, columns(peer(dh, 0))])
-        c_near_eo[i].wait_recv()
-        far_send[i] = (part + near_recv[i].astype(f32)).astype(bf16)
-        c_far.append(send(far_send.at[i], far_recv.at[i], (ep, peer(dh, 0))))
-    part = matmul(e_hid[...], ed[:, own])
-    c_near_eo[half - 1].wait_recv()
-    eo_own[...] = part + near_recv[half - 1].astype(f32)
-    loads[5].wait()
-    for copy in c_hid_near:
-        copy.wait_recv()
-    hidden = d_hid[...].reshape(n_ep * tokens, units)
-    d_out[...] = matmul(hidden, ddw[...]).reshape(d_out.shape)
-    total = eo_own[...]
-    for i in range(half - 1):
-        c_far[i].wait_recv()
-        total = total + far_recv[i].astype(f32)
-    eo_own[...] = total
+                pick(partner, t, r, other)
+                block = member(t, r)
+                chosen = sel_recv[block].astype(f32)
+                masked = jnp.where(chosen_lane < tokens, chosen * scale_rows[block, 0:1, :], 0.0)
+                column = jnp.sum(masked, axis=1, keepdims=True)
+                at = slice((2 * t + r) * cap, (2 * t + r + 1) * cap)
+                row_scale[at, :] = jnp.broadcast_to(column, (cap, lanes))
+
+    inner_width = eg.shape[1]
+    tile = 256 if inner_width % 256 == 0 else 128
+
+    def expert_in(p):
+        for t in parts[p]:
+            for dh in range(1, half):
+                c_pass[t, dh].wait_recv()
+        at = slice(p * count, (p + 1) * count)
+
+        scale = row_scale[at, 0:1]
+        for i in range(inner_width // tile):
+            cols = slice(i * tile, (i + 1) * tile)
+            gate_part = matmul(rows_all[0, at], eg[0:quarter, cols])
+            up_part = matmul(rows_all[0, at], eu[0:quarter, cols])
+            for q in range(1, n_tp):
+                span = slice(q * quarter, (q + 1) * quarter)
+                gate_part = gate_part + matmul(rows_all[q, at], eg[span, cols])
+                up_part = up_part + matmul(rows_all[q, at], eu[span, cols])
+            e_hid[at, cols] = (silu(gate_part * scale) * (up_part * scale)).astype(bf16)
+
+    def expert_near(p):
+        at = slice(p * count, (p + 1) * count)
+        for i, dh in enumerate(list(range(1, half)) + [0]):
+            near_send[p, i] = matmul(e_hid[at, :], ed[:, columns(peer(dh, 1))]).astype(bf16)
+            source, target = near_send.at[p, i], near_recv.at[p, i]
+            c_eo_near[p, i] = send(source, target, (ep, partner))
+
+    def expert_far(p):
+        at = slice(p * count, (p + 1) * count)
+        for i, dh in enumerate(range(1, half)):
+            part = matmul(e_hid[at, :], ed[:, columns(peer(dh, 0))])
+            c_eo_near[p, i].wait_recv()
+            far_send[p, i] = (part + near_recv[p, i].astype(f32)).astype(bf16)
+            source, target = far_send.at[p, i], far_recv.at[p, i]
+            c_eo_far[p, i] = send(source, target, (ep, peer(dh, 0)))
+        part = matmul(e_hid[at, :], ed[:, own])
+        c_eo_near[p, half - 1].wait_recv()
+        eo_own[at, :] = part + near_recv[p, half - 1].astype(f32)
+
+    def expert_total(p):
+        at = slice(p * count, (p + 1) * count)
+        total = eo_own[at, :]
+        for i in range(half - 1):
+            c_eo_far[p, i].wait_recv()
+            total = total + far_recv[p, i].astype(f32)
+        eo_own[at, :] = total
 
     def outcome(t, r):
         block = member(t, r)
@@ -375,25 +346,98 @@
         routed = lax.dot_general(
             chosen[:, :tokens], answers, (((0,), (0,)), ((), ())), preferred_element_type=f32
         )
-        branch = column_of(scale_rows[block, 1:2, :])
-        return branch * d_out[(t % half) * 2 + r, t // half] + routed
-
-    order = list(range(1, n_z)) + [0]
-    c_y = {}
-    for t in order:
-        y_send[t] = outcome(t, 1).astype(bf16)
-        c_y[t] = send(y_send.at[t], y_recv.at[t], (near, tp))
-    c_out = []
-    for t in order:
-        mine = outcome(t, 0)
-        c_y[t].wait_recv()
-        mine = mine + y_recv[t].astype(f32)
-        if t:
-            z_send[t - 1] = mine.astype(bf16)
-            c_out.append(send(z_send.at[t - 1], z_recv.at[t - 1], (member(t, 0), tp)))
-    mine = mine + mid_buf[...]
+        branch = jnp.sum(eye * scale_rows[block, 1:2, :], axis=1, keepdims=True)
+        p, k = t // per_part, t % per_part
+        dense = [d_out[p, 2 * j + r, k * sub : (k + 1) * sub, :] for j in range(half)]
+        return branch * jnp.concatenate(dense, axis=0) + routed
+
+    def far_first(p):
+        return [t for t in parts[p] if t] + [t for t in parts[p] if not t]
+
+    def send_near(p):
+        for t in far_first(p):
+            y_send[t] = outcome(t, 1).astype(bf16)
+            c_y[t] = send(y_send.at[t], y_recv.at[t], (near, tp))
+
+    def send_out(p):
+        for t in far_first(p):
+            mine = outcome(t, 0)
+            c_y[t].wait_recv()
+            mine = mine + y_recv[t].astype(f32)
+            if t:
+                z_send[t - 1] = mine.astype(bf16)
+                c_out[t] = send(z_send.at[t - 1], z_recv.at[t - 1], (member(t, 0), tp))
+            else:
+                mid_buf[...] = mid_buf[...] + mine
+
+    share(0, 0)
+    for copy in c_sel:
+        copy.wait_recv()
+    pick(tp, 0, 0, piece)
+    c_near.wait_recv()
+    share(0, 1)
+    pick(tp, 0, 1, piece)
+    send_rows(0)
+    c_relay = [None]
     for t in range(1, n_z):
-        c_out[t - 1].wait_recv()
+        c_z[t].wait_recv()
+        block = member(t, 0)
+        c_relay.append(send(piece.at[block], piece.at[block], (near, tp)))
+        share(t, 0)
+        pick(tp, t, 0, piece)
+        if t == 1:
+            loads[0].wait()
+            loads[1].wait()
+            for copy in c_dense:
+                copy.wait_recv()
+            partial(0)
+    for copy in c_stat:
+        copy.wait_recv()
+    c_total = []
+    for dh, dc in peers:
+        c_total.append(send(stat.at[tp], stat.at[tp], (ep, peer(dh, dc))))
+    for t in range(1, n_z):
+        c_relay[t].wait_recv()
+        share(t, 1)
+        pick(tp, t, 1, piece)
+        send_rows(t)
+        if t > 1:
+            partial(t - 1)
+        if t != 2:
+            pass_rows(max(t - 2, 0))
+    scales()
+    prepare(0)
+    for t in range(max(n_z - 2, 1), per_part):
+        pass_rows(t)
+    partial(n_z - 1)
+    loads[2].wait()
+    loads[3].wait()
+    expert_in(0)
+    for t in range(max(n_z - 2, per_part), n_z):
+        pass_rows(t)
+    loads[4].wait()
+    expert_near(0)
+    activate(0)
+    prepare(1)
+    expert_far(0)
+    activate(1)
+    expert_in(1)
+    expert_near(1)
+    pass_hidden(0)
+    expert_far(1)
+    loads[5].wait()
+    dense_down(0)
+    expert_total(0)
+    send_near(0)
+    pass_hidden(1)
+    dense_down(1)
+    expert_total(1)
+    send_near(1)
+    send_out(0)
+    send_out(1)
+    mine = mid_buf[...]
+    for t in range(1, n_z):
+        c_out[t].wait_recv()
         mine = mine + z_recv[t - 1].astype(f32)
     mixed_ref[...] = mine.astype(bf16)
     for copy in sent:
@@ -407,7 +451,8 @@
     cap, lanes = sel.shape[1:]
     items = n_ep * cap
     n_z, half = n_ep // 2, n_tp // 2
-    groups = n_z // half
+    sub = tokens // half
+    part = items // 2
     units = dg.shape[1]
     bf16, f32 = jnp.bfloat16, jnp.float32
     vmem = pl.BlockSpec(memory_space=pltpu.VMEM)
@@ -430,17 +475,17 @@
         pltpu.VMEM((n_ep, tokens, quarter), bf16),
         pltpu.VMEM((n_tp, items, quarter), bf16),
         pltpu.VMEM((items, lanes), f32),
-        pltpu.VMEM((groups, half - 1, 2, tokens, units), bf16),
-        pltpu.VMEM((groups, half - 1, 2, tokens, units), bf16),
-        pltpu.VMEM((groups, 2, tokens, units), f32),
+        pltpu.VMEM((n_z, half - 1, 2, sub, units), bf16),
+        pltpu.VMEM((n_z, half - 1, 2, sub, units), bf16),
+        pltpu.VMEM((n_z, 2, sub, units), f32),
         pltpu.VMEM((items, eg.shape[1]), bf16),
-        pltpu.VMEM((half, items, quarter), bf16),
-        pltpu.VMEM((half, items, quarter), bf16),
-        pltpu.VMEM((half - 1, items, quarter), bf16),
-        pltpu.VMEM((half - 1, items, quarter), bf16),
+        pltpu.VMEM((2, half, part, quarter), bf16),
+        pltpu.VMEM((2, half, part, quarter), bf16),
+        pltpu.VMEM((2, half - 1, part, quarter), bf16),
+        pltpu.VMEM((2, half - 1, part, quarter), bf16),
         pltpu.VMEM((items, quarter), f32),
-        pltpu.VMEM((n_tp, groups, tokens, units), bf16),
-        pltpu.VMEM((n_tp, groups, tokens, quarter), f32),
+        pltpu.VMEM((n_tp, 2, n_z // 2 * sub, units), bf16),
+        pltpu.VMEM((2, n_tp, n_z // 2 * sub, quarter), f32),
         pltpu.VMEM((n_z, tokens, quarter), bf16),
         pltpu.VMEM((n_z, tokens, quarter), bf16),
         pltpu.VMEM((n_z - 1, tokens, quarter), bf16),

time: 60.1 us -> 56.2 us (0.935)
  Pallas kernels: 57.8 us -> 53.9 us
    pallas_call x1, Pallas kernels: 47.9 us -> 44.1 us  [run_layer(): pl.pallas_call(functools.partial(layer_kernel, n_ep, n_tp), out_shape=jax...]
where the time goes in v3:
time: 56.2 us; the launch traced here: 56 us
  Pallas kernels  53.9 us (96%)
  local copies, waits for them, and re-layouts  1.42 us (3%)
  between operations  0.65 us (1%)
    pallas_call x1, Pallas kernels, run_layer(): pl.pallas_call(functools.partial(layer_kernel, n_ep, n_tp), out_shape=jax...  44.1 us
    pallas_call x1, Pallas kernels, run_attention(): pl.pallas_call(functools.partial(attention_kernel, cap), out_shape=(jax.S...  9.84 us
    unnamed x1, local copies, waits for them, and re-layouts  1.42 us

profile of v3, /device:TPU:0, one launch (start us, length us, event | category | flops | bytes accessed | tf_op | source)
XLA Modules:
  0.0 56.0 jit_solution(12907243000204099957)
XLA Ops:
  0.6 9.8 %shard_map.212 = (bf16[48,256]{1,0:T(8,128)(2,1)}, bf16[128,128]{1,0:T(8,128)(2,1)}, f32[48,1,128,256]{3,2,1,0:T(8,128)}) custom-call(bf16[48,2048]{1,0:T(8,128)(2,1)} %hid_ref.1, bf16[16,128]{1,0:T(8,128)(2,1)} %bitcast.13, f32[48,128]{1,0:T(8,128)} %shift_ref.1, bf16[1,256]{1,0:T(2,128)(2,1)} %head_gain_ref.1, s32[2,48]{1,0:T(2,128)} %bitcast.16, ...), custom_call_target="tpu_custom_call" | custom-call | tf_op jit(solution)/shard_map/pallas_call | solution.py:645
  10.5 44.1 %shard_map.213 = bf16[48,512]{1,0:T(8,128)(2,1)} custom-call(bf16[48,256]{1,0:T(8,128)(2,1)} %get-tuple-element.5.gated_ref, bf16[256,2048]{1,0:T(8,128)(2,1)} %outw_ref.1, bf16[48,2048]{1,0:T(8,128)(2,1)} %hid_ref.1, bf16[16,128]{1,0:T(8,128)(2,1)} %bitcast.14, bf16[16,128]{1,0:T(8,128)(2,1)} %bitcast.15, bf16[8,16,128]{2,1,0:T(8,128)(2,1)} %bitcast.12, ...), custom_call_target="tpu_custom_call" | custom-call | tf_op jit(solution)/shard_map/pallas_call | solution.py:497
  54.6 1.4 %copy.24 = bf16[48,512]{1,0:T(8,128)(2,1)} copy(bf16[48,512]{1,0:T(8,128)(2,1)} %shard_map.213) | data formatting | bytes 98304

commit v4 on v3

--- a/solution.py
+++ b/solution.py
@@ -23,6 +23,10 @@
 def flat_row(ref):
     rows = ref[...].astype(jnp.float32)
     return jnp.concatenate([rows[k : k + 1, :] for k in range(rows.shape[0])], axis=1)
+
+
+def in_hbm(array):
+    return pltpu.with_memory_space_constraint(array, pltpu.HBM)
 
 
 def silu(values):
@@ -501,36 +505,43 @@
         out_specs=vmem,
         scratch_shapes=scratch,
         compiler_params=pltpu.CompilerParams(
-            collective_id=0, has_side_effects=True, vmem_limit_bytes=60 * 1024 * 1024
+            collective_id=0, has_side_effects=True, vmem_limit_bytes=36 * 1024 * 1024
         ),
-    )(gated, output_weight, hid, gain, gate, sel, eg, eu, ed, dg, du, dd)
+    )(gated, output_weight, hid, gain, gate, sel, *map(in_hbm, (eg, eu, ed, dg, du, dd)))
 
 
 def attention_kernel(
     cap,
-    hidden_ref,
-    gain_ref,
-    shift_ref,
-    head_gain_ref,
-    routes_ref,
-    weights_ref,
+    hidden_hbm,
+    gain_hbm,
+    shift_hbm,
+    head_gain_hbm,
+    routes_hbm,
+    weights_hbm,
     qw_hbm,
     kw_hbm,
     vw_hbm,
     ow_hbm,
     fw_hbm,
     state_hbm,
+    outw_hbm,
     gated_ref,
     sel_ref,
+    hidden_ref,
+    outw_ref,
     new_hbm,
+    gain_ref,
+    shift_ref,
+    head_gain_ref,
+    routes_ref,
+    weights_ref,
     qw,
     kw,
     vw,
     ow,
     fw,
     state,
-    query,
-    key,
+    key_query,
     value,
     decay,
     readout,
@@ -539,15 +550,28 @@
     out_sem,
 ):
     f32, bf16 = jnp.float32, jnp.bfloat16
-    tokens = hidden_ref.shape[0]
+    tokens = hidden_hbm.shape[0]
     heads, key_dim, value_dim = state.shape[1:]
     groups = tokens // 8
     loads = []
-    pairs = ((fw_hbm, fw), (kw_hbm, kw), (qw_hbm, qw), (vw_hbm, vw), (ow_hbm, ow))
+    pairs = (
+        (fw_hbm, fw),
+        (kw_hbm, kw),
+        (qw_hbm, qw),
+        (vw_hbm, vw),
+        (ow_hbm, ow),
+        (hidden_hbm, hidden_ref),
+        (gain_hbm, gain_ref),
+        (routes_hbm, routes_ref),
+        (weights_hbm, weights_ref),
+        (shift_hbm, shift_ref),
+        (head_gain_hbm, head_gain_ref),
+        (outw_hbm, outw_ref),
+    )
     for i, (src, dst) in enumerate(pairs):
-        load = pltpu.make_async_copy(src, dst, w_sem.at[i])
-        load.start()
-        loads.append(load)
+        loads.append(pltpu.make_async_copy(src, dst, w_sem.at[i]))
+    for i in (5, 6, 0, 1, 2, 3, 7, 8, 9, 10):
+        loads[i].start()
 
     def fetch(g):
         rows = pl.ds(g * 8, 8)
@@ -557,12 +581,17 @@
         rows = pl.ds(g * 8, 8)
         return pltpu.make_async_copy(state.at[rows], new_hbm.at[rows], out_sem.at[g])
 
+    loads[5].wait()
     for g in range(groups):
         fetch(g).start()
-
+    loads[4].start()
+    loads[11].start()
+    loads[6].wait()
     inputs = hidden_ref[...].astype(f32)
     normed = (inputs * rms_factor(inputs) * flat_row(gain_ref)).astype(bf16)
 
+    loads[7].wait()
+    loads[8].wait()
     items, lanes = sel_ref.shape
     experts = (items // cap + 7) // 8 * 8
     first, second = routes_ref[0:1, :], routes_ref[1:2, :]
@@ -590,15 +619,21 @@
         return matmul(normed, weight[...]).astype(bf16).astype(f32)
 
     loads[0].wait()
+    loads[9].wait()
+    loads[10].wait()
     drive = matmul(normed, fw[...])
     log_sig = jnp.minimum(drive, 0.0) - jnp.log1p(jnp.exp(-jnp.abs(drive)))
     decay[...] = jnp.exp(log_sig / TAU_DECAY + shift_ref[...]).reshape(decay.shape)
     loads[1].wait()
-    key[...] = rounded_rows(kw).reshape(key.shape)
+    key_query[:, 0:8] = rounded_rows(kw).reshape(decay.shape)
     loads[2].wait()
-    query[...] = (rounded_rows(qw) * key_dim ** (-0.5)).reshape(query.shape)
+    key_query[:, 8:16] = rounded_rows(qw).reshape(decay.shape)
     loads[3].wait()
     value[...] = rounded_rows(vw).reshape(value.shape)
+    spread_width = value_dim + 128
+    token = lax.broadcasted_iota(jnp.int32, (16, spread_width), 0)
+    column = lax.broadcasted_iota(jnp.int32, (16, spread_width), 1)
+    unit = jnp.ones((1, 128), f32)
 
     @pl.loop(0, groups)
     def _(g):
@@ -607,32 +642,34 @@
             keys = slice(h * key_dim, (h + 1) * key_dim)
             vals = slice(h * value_dim, (h + 1) * value_dim)
             decay_cols = jnp.transpose(decay[g, :, keys])
-            key_cols = jnp.transpose(key[g, :, keys])
-            query_cols = jnp.transpose(query[g, :, keys])
+            left = jnp.transpose(key_query[g, :, keys]).astype(bf16)
             for j in range(8):
-                fresh = (
-                    decay_cols[:, j : j + 1] * state[g * 8 + j, h]
-                    + key_cols[:, j : j + 1] * value[g, j : j + 1, vals]
-                )
+                right = jnp.concatenate([value[g, j : j + 1, vals], unit], axis=1)
+                wanted = token == jnp.where(column < value_dim, j, 8 + j)
+                products = matmul(left, jnp.where(wanted, right, 0.0).astype(bf16))
+                fresh = decay_cols[:, j : j + 1] * state[g * 8 + j, h] + products[:, :value_dim]
                 state[g * 8 + j, h] = fresh
-                readout[g, j : j + 1, vals] = jnp.sum(
-                    query_cols[:, j : j + 1] * fresh, axis=0, keepdims=True
-                )
+                asked = products[:, value_dim:]
+                asked = jnp.concatenate([asked] * (value_dim // 128), axis=1)
+                readout[g, j : j + 1, vals] = jnp.sum(asked * fresh, axis=0, keepdims=True)
         put(g).start()
 
     loads[4].wait()
     outgate = rounded_rows(ow)
-    out = readout[...].reshape(tokens, heads * value_dim)
+    out = readout[...].reshape(tokens, heads * value_dim) * key_dim ** (-0.5)
     for h in range(heads):
         vals = slice(h * value_dim, (h + 1) * value_dim)
         part = out[:, vals]
         gain = head_gain_ref[:, vals].astype(f32)
         gated_ref[:, vals] = (part * rms_factor(part) * gain * silu(outgate[:, vals])).astype(bf16)
+    loads[11].wait()
     for g in range(groups):
         put(g).wait()
 
 
-def run_attention(hidden, gain, shift, head_gain, routes, weights, qw, kw, vw, ow, fw, state, n_ep):
+def run_attention(
+    hidden, gain, shift, head_gain, routes, weights, qw, kw, vw, ow, fw, state, outw, n_ep
+):
     bf16, f32 = jnp.bfloat16, jnp.float32
     tokens, heads, key_dim, value_dim = state.shape
     capacity = tokens * routes.shape[0] // n_ep + 2
@@ -642,30 +679,32 @@
     lanes = (tokens + 2 + 127) // 128 * 128
     vmem = pl.BlockSpec(memory_space=pltpu.VMEM)
     anyspace = pl.BlockSpec(memory_space=pl.ANY)
-    gated, sel, new_state = pl.pallas_call(
+    operands = (hidden, gain, shift, head_gain, routes, weights, qw, kw, vw, ow, fw, state, outw)
+    gated, sel, hidden, outw, new_state = pl.pallas_call(
         functools.partial(attention_kernel, cap),
         out_shape=(
-            jax.ShapeDtypeStruct((tokens, heads * value_dim), bf16),
-            jax.ShapeDtypeStruct((items, lanes), bf16),
+            pltpu.VMEM((tokens, heads * value_dim), bf16),
+            pltpu.VMEM((items, lanes), bf16),
+            pltpu.VMEM(hidden.shape, bf16),
+            pltpu.VMEM(outw.shape, bf16),
             jax.ShapeDtypeStruct(state.shape, f32),
         ),
-        in_specs=[vmem] * 6 + [anyspace] * 6,
-        out_specs=(vmem, vmem, anyspace),
-        scratch_shapes=[pltpu.VMEM(w.shape, bf16) for w in (qw, kw, vw, ow, fw)]
+        in_specs=[anyspace] * 13,
+        out_specs=(vmem, vmem, vmem, vmem, anyspace),
+        scratch_shapes=[pltpu.VMEM(a.shape, a.dtype) for a in operands[1:11]]
         + [
             pltpu.VMEM(state.shape, f32),
-            pltpu.VMEM((groups, 8, heads * key_dim), f32),
-            pltpu.VMEM((groups, 8, heads * key_dim), f32),
+            pltpu.VMEM((groups, 16, heads * key_dim), f32),
             pltpu.VMEM((groups, 8, heads * value_dim), f32),
             pltpu.VMEM((groups, 8, heads * key_dim), f32),
             pltpu.VMEM((groups, 8, heads * value_dim), f32),
-            pltpu.SemaphoreType.DMA((5,)),
+            pltpu.SemaphoreType.DMA((12,)),
             pltpu.SemaphoreType.DMA((groups,)),
             pltpu.SemaphoreType.DMA((groups,)),
         ],
-        compiler_params=pltpu.CompilerParams(vmem_limit_bytes=60 * 1024 * 1024),
-    )(hidden, gain, shift, head_gain, routes, weights, qw, kw, vw, ow, fw, state)
-    return gated, sel.reshape(n_ep, cap, lanes), new_state
+        compiler_params=pltpu.CompilerParams(vmem_limit_bytes=24 * 1024 * 1024),
+    )(*map(in_hbm, operands))
+    return gated, sel.reshape(n_ep, cap, lanes), hidden, outw, new_state
 
 
 def body(
@@ -691,7 +730,7 @@
     dense_up,
     dense_down,
 ):
-    gated, sel, new_state = run_attention(
+    gated, sel, hidden, outw, new_state = run_attention(
         hidden_in,
         input_gain.reshape(-1, 128),
         decay_shift,
@@ -704,12 +743,13 @@
         outgate_weight,
         decay_weight,
         carried_state,
+        output_weight,
         lax.axis_size("ep"),
     )
     mixed = run_layer(
         gated,
-        output_weight,
-        hidden_in,
+        outw,
+        hidden,
         channel_gain.reshape(-1, 128),
         branch_gate.reshape(-1, 128),
         sel,

time: 56.2 us -> 50.3 us (0.90)
  Pallas kernels: 53.9 us -> 48.9 us
  local copies, waits for them, and re-layouts: 1.42 us -> 0.63 us
    pallas_call x1, Pallas kernels: 9.84 us -> 6.69 us  [run_attention(): pl.pallas_call(functools.partial(attention_kernel, cap), out_shape=(pltpu...]
    pallas_call x1, Pallas kernels: 44.1 us -> 42.2 us  [run_layer(): pl.pallas_call(functools.partial(layer_kernel, n_ep, n_tp), out_shape=jax...]
    unnamed x1 -> x5, local copies, waits for them, and re-layouts: 1.42 us -> 0.63 us
where the time goes in v4:
time: 50.3 us; the launch traced here: 50.2 us
  Pallas kernels  48.9 us (97%)
  between operations  0.68 us (1%)
  local copies, waits for them, and re-layouts  0.63 us (1%)
    pallas_call x1, Pallas kernels, run_layer(): pl.pallas_call(functools.partial(layer_kernel, n_ep, n_tp), out_shape=jax...  42.2 us
    pallas_call x1, Pallas kernels, run_attention(): pl.pallas_call(functools.partial(attention_kernel, cap), out_shape=(pltpu...  6.69 us

profile of v4, /device:TPU:0, one launch (start us, length us, event | category | flops | bytes accessed | tf_op | source)
XLA Modules:
  0.0 50.2 jit_solution(7741996558152583526)
XLA Ops:
  0.6 0.0 copy-start
  0.6 0.0 copy-start.1
  0.7 6.7 %shard_map.212 = (bf16[48,256]{1,0:T(8,128)(2,1)S(1)}, bf16[128,128]{1,0:T(8,128)(2,1)S(1)}, bf16[48,2048]{1,0:T(8,128)(2,1)S(1)}, bf16[256,2048]{1,0:T(8,128)(2,1)S(1)}, f32[48,1,128,256]{3,2,1,0:T(8,128)}) custom-call(bf16[48,2048]{1,0:T(8,128)(2,1)} %hidden_hbm.1, bf16[16,128]{1,0:T(8,128)(2,1)} %bitcast.15, f32[48,128]{1,0:T(8,128)} %shift_hbm.1, ...), custom_call_target="tpu_custom_call" | custom-call | tf_op jit(solution)/shard_map/pallas_call | solution.py:683
  7.4 0.0 copy-done
  7.4 0.0 copy-done.1
  7.4 42.2 %shard_map.213 = bf16[48,512]{1,0:T(8,128)(2,1)S(1)} custom-call(bf16[48,256]{1,0:T(8,128)(2,1)S(1)} %get-tuple-element.7.gated_ref, bf16[256,2048]{1,0:T(8,128)(2,1)S(1)} %get-tuple-element.8.outw_ref, bf16[48,2048]{1,0:T(8,128)(2,1)S(1)} %get-tuple-element.9.hid_ref, bf16[16,128]{1,0:T(8,128)(2,1)S(1)} %bitcast.10, bf16[16,128]{1,0:T(8,128)(2,1)S(1)} %bitcast.11, ...), custom_call_target="tpu_custom_call" | custom-call | tf_op jit(solution)/shard_map/pallas_call | solution.py:501
  49.6 0.6 %copy.24 = bf16[48,512]{1,0:T(8,128)(2,1)} copy(bf16[48,512]{1,0:T(8,128)(2,1)S(1)} %shard_map.213) | data formatting | bytes 98304
Async XLA Ops:
  0.6 6.7 %copy-start = (bf16[2048]{0:T(1024)(128)(2,1)S(1)}, bf16[2048]{0:T(1024)(128)(2,1)}, u32[]{:S(2)}) copy-start(bf16[2048]{0:T(1024)(128)(2,1)} %param.32) | copy-start | bytes 12292
  0.6 6.7 %copy-start.1 = (bf16[2048]{0:T(1024)(128)(2,1)S(1)}, bf16[2048]{0:T(1024)(128)(2,1)}, u32[]{:S(2)}) copy-start(bf16[2048]{0:T(1024)(128)(2,1)} %param.33) | copy-start | bytes 12292

commit v5 on v4

--- a/solution.py
+++ b/solution.py
@@ -97,14 +97,23 @@
     h, c = lax.div(tp, 2), lax.rem(tp, 2)
     partner = tp + 1 - 2 * c
     near = ep + 1 - 2 * lax.rem(ep, 2)
-    steps = [0] + sorted(range(1, n_z), key=lambda m: abs(m - n_z // 2))
+    steps = list(range(n_z))
+    mirrored = n_z & (n_z - 1) == 0
     own = pl.ds(pl.multiple_of(tp * quarter, quarter), quarter)
 
     def columns(q):
         return pl.ds(pl.multiple_of(q * quarter, quarter), quarter)
 
-    def member(t, r):
-        return lax.rem((near if r else ep) - 2 * steps[t] + n_ep, n_ep)
+    def member(t, r, ahead=False):
+        base, step = near if r else ep, steps[t]
+        if not mirrored:
+            return lax.rem(base + (2 * step if ahead else n_ep - 2 * step), n_ep)
+        target, bit = lax.rem(base, 2), 1
+        while bit < n_z:
+            digit = lax.rem(lax.div(base, 2 * bit), 2)
+            target = target + 2 * bit * (1 - digit if step & bit else digit)
+            bit *= 2
+        return target
 
     def peer(dh, dc):
         return lax.rem(h + dh, half) * 2 + lax.rem(c + dc, 2)
@@ -167,6 +176,12 @@
     middle = (hid_ref[:, own].astype(f32) + attended).astype(bf16).astype(f32)
     shaped = middle * gain_row[:, own]
     piece[ep] = shaped.astype(bf16)
+    c_near = send(piece.at[ep], piece.at[ep], (near, tp))
+    sides = [pl.ds(k * quarter // 2, quarter // 2) for k in range(2)]
+    c_z = [None]
+    for t in range(1, n_z):
+        target = member(t, 0, ahead=True)
+        c_z.append([send(piece.at[ep, :, k], piece.at[ep, :, k], (target, tp)) for k in sides])
     squares = jnp.sum(middle * middle, axis=-1, keepdims=True)
     inner = jnp.sum(shaped * gate_row[:, own], axis=-1, keepdims=True)
     line = lax.broadcasted_iota(jnp.int32, (tokens, lanes), 0)
@@ -174,15 +189,10 @@
     eye = jnp.where(line == lane, 1.0, 0.0)
     stat[tp, ep, 0:1, :] = jnp.sum(eye * squares, axis=0, keepdims=True)
     stat[tp, ep, 1:2, :] = jnp.sum(eye * inner, axis=0, keepdims=True)
-    c_near = send(piece.at[ep], piece.at[ep], (near, tp))
     c_stat = []
     for d in range(1, n_ep):
         target = lax.rem(ep + d, n_ep)
         c_stat.append(send(stat.at[tp, ep], stat.at[tp, ep], (target, tp)))
-    c_z = [None]
-    for t in range(1, n_z):
-        target = lax.rem(ep + 2 * steps[t], n_ep)
-        c_z.append(send(piece.at[ep], piece.at[ep], (target, tp)))
     mid_buf[...] = middle
 
     c_other = {}
@@ -226,7 +236,7 @@
     def partial(t):
         for r in range(2):
             c_other[t, r].wait_recv()
-        block = lax.rem(jnp.where(c == 1, near, ep) - 2 * steps[t] + n_ep, n_ep)
+        block = jnp.where(c == 1, member(t, 1), member(t, 0))
         left, right = piece[block], other[block]
         for i, w in enumerate((wg, wu)):
             product = matmul(left, w[c]) + matmul(right, w[1 - c])
@@ -248,7 +258,7 @@
                 c_gu[t, dh].wait_recv()
                 gate_sum = gate_sum + gu_recv[t, dh - 1, 0].astype(f32)
                 up_sum = up_sum + gu_recv[t, dh - 1, 1].astype(f32)
-            block = lax.rem(jnp.where(c == 1, near, ep) - 2 * steps[t] + n_ep, n_ep)
+            block = jnp.where(c == 1, member(t, 1), member(t, 0))
             scale = jnp.sum(eye_own * scale_rows[block, 0:1, :], axis=1, keepdims=True)
             shares.append(silu(gate_sum * scale) * (up_sum * scale))
         d_hid[tp, p] = jnp.concatenate(shares, axis=0).astype(bf16)
@@ -320,24 +330,33 @@
             source, target = near_send.at[p, i], near_recv.at[p, i]
             c_eo_near[p, i] = send(source, target, (ep, partner))
 
+    def far_first(p):
+        return [t for t in parts[p] if t] + [t for t in parts[p] if not t]
+
     def expert_far(p):
         at = slice(p * count, (p + 1) * count)
         for i, dh in enumerate(range(1, half)):
             part = matmul(e_hid[at, :], ed[:, columns(peer(dh, 0))])
             c_eo_near[p, i].wait_recv()
             far_send[p, i] = (part + near_recv[p, i].astype(f32)).astype(bf16)
-            source, target = far_send.at[p, i], far_recv.at[p, i]
-            c_eo_far[p, i] = send(source, target, (ep, peer(dh, 0)))
+            for t in far_first(p):
+                rows = pl.ds(2 * (t % per_part) * cap, 2 * cap)
+                source, target = far_send.at[p, i, rows], far_recv.at[p, i, rows]
+                c_eo_far[t, i] = send(source, target, (ep, peer(dh, 0)))
+
+    def expert_own(p):
+        at = slice(p * count, (p + 1) * count)
         part = matmul(e_hid[at, :], ed[:, own])
         c_eo_near[p, half - 1].wait_recv()
         eo_own[at, :] = part + near_recv[p, half - 1].astype(f32)
 
-    def expert_total(p):
-        at = slice(p * count, (p + 1) * count)
+    def expert_total(t):
+        at = slice(2 * t * cap, 2 * (t + 1) * cap)
+        p, k = t // per_part, t % per_part
         total = eo_own[at, :]
         for i in range(half - 1):
-            c_eo_far[p, i].wait_recv()
-            total = total + far_recv[p, i].astype(f32)
+            c_eo_far[t, i].wait_recv()
+            total = total + far_recv[p, i, 2 * k * cap : 2 * (k + 1) * cap].astype(f32)
         eo_own[at, :] = total
 
     def outcome(t, r):
@@ -355,24 +374,28 @@
         dense = [d_out[p, 2 * j + r, k * sub : (k + 1) * sub, :] for j in range(half)]
         return branch * jnp.concatenate(dense, axis=0) + routed
 
-    def far_first(p):
-        return [t for t in parts[p] if t] + [t for t in parts[p] if not t]
+    halves = [slice(k * quarter // 2, (k + 1) * quarter // 2) for k in range(2)]
 
     def send_near(p):
         for t in far_first(p):
-            y_send[t] = outcome(t, 1).astype(bf16)
-            c_y[t] = send(y_send.at[t], y_recv.at[t], (near, tp))
-
-    def send_out(p):
-        for t in far_first(p):
+            expert_total(t)
+            mine = outcome(t, 1).astype(bf16)
+            for k in range(2):
+                y_send[t, k] = mine[:, halves[k]]
+                c_y[t, k] = send(y_send.at[t, k], y_recv.at[t, k], (near, tp))
+
+    def send_out(ts):
+        for t in ts:
             mine = outcome(t, 0)
-            c_y[t].wait_recv()
-            mine = mine + y_recv[t].astype(f32)
-            if t:
-                z_send[t - 1] = mine.astype(bf16)
-                c_out[t] = send(z_send.at[t - 1], z_recv.at[t - 1], (member(t, 0), tp))
-            else:
-                mid_buf[...] = mid_buf[...] + mine
+            for k in range(2):
+                c_y[t, k].wait_recv()
+                total = mine[:, halves[k]] + y_recv[t, k].astype(f32)
+                if t:
+                    z_send[t - 1, k] = total.astype(bf16)
+                    source, target = z_send.at[t - 1, k], z_recv.at[t - 1, k]
+                    c_out[t, k] = send(source, target, (member(t, 0), tp))
+                else:
+                    mid_buf[:, halves[k]] = mid_buf[:, halves[k]] + total
 
     share(0, 0)
     for copy in c_sel:
@@ -384,9 +407,11 @@
     send_rows(0)
     c_relay = [None]
     for t in range(1, n_z):
-        c_z[t].wait_recv()
         block = member(t, 0)
-        c_relay.append(send(piece.at[block], piece.at[block], (near, tp)))
+        c_relay.append([])
+        for copy, k in zip(c_z[t], sides):
+            copy.wait_recv()
+            c_relay[t].append(send(piece.at[block, :, k], piece.at[block, :, k], (near, tp)))
         share(t, 0)
         pick(tp, t, 0, piece)
         if t == 1:
@@ -395,32 +420,34 @@
             for copy in c_dense:
                 copy.wait_recv()
             partial(0)
-    for copy in c_stat:
-        copy.wait_recv()
     c_total = []
-    for dh, dc in peers:
-        c_total.append(send(stat.at[tp], stat.at[tp], (ep, peer(dh, dc))))
     for t in range(1, n_z):
-        c_relay[t].wait_recv()
+        for copy in c_relay[t]:
+            copy.wait_recv()
         share(t, 1)
         pick(tp, t, 1, piece)
         send_rows(t)
+        if t == 1:
+            for copy in c_stat:
+                copy.wait_recv()
+            for dh, dc in peers:
+                c_total.append(send(stat.at[tp], stat.at[tp], (ep, peer(dh, dc))))
         if t > 1:
             partial(t - 1)
         if t != 2:
             pass_rows(max(t - 2, 0))
+    partial(n_z - 1)
     scales()
     prepare(0)
     for t in range(max(n_z - 2, 1), per_part):
         pass_rows(t)
-    partial(n_z - 1)
     loads[2].wait()
     loads[3].wait()
     expert_in(0)
+    loads[4].wait()
+    expert_near(0)
     for t in range(max(n_z - 2, per_part), n_z):
         pass_rows(t)
-    loads[4].wait()
-    expert_near(0)
     activate(0)
     prepare(1)
     expert_far(0)
@@ -428,22 +455,24 @@
     expert_in(1)
     expert_near(1)
     pass_hidden(0)
+    expert_own(0)
     expert_far(1)
+    pass_hidden(1)
+    expert_own(1)
     loads[5].wait()
     dense_down(0)
-    expert_total(0)
     send_near(0)
-    pass_hidden(1)
     dense_down(1)
-    expert_total(1)
     send_near(1)
-    send_out(0)
-    send_out(1)
-    mine = mid_buf[...]
-    for t in range(1, n_z):
-        c_out[t].wait_recv()
-        mine = mine + z_recv[t - 1].astype(f32)
-    mixed_ref[...] = mine.astype(bf16)
+    send_out(range(1, per_part))
+    send_out(range(per_part, n_z))
+    send_out([0])
+    for k in range(2):
+        mine = mid_buf[:, halves[k]]
+        for t in range(1, n_z):
+            c_out[t, k].wait_recv()
+            mine = mine + z_recv[t - 1, k].astype(f32)
+        mixed_ref[:, halves[k]] = mine.astype(bf16)
     for copy in sent:
         copy.wait_send()
 
@@ -461,7 +490,7 @@
     bf16, f32 = jnp.bfloat16, jnp.float32
     vmem = pl.BlockSpec(memory_space=pltpu.VMEM)
     anyspace = pl.BlockSpec(memory_space=pl.ANY)
-    copies = 8 * n_ep + 4 * n_tp + 6 * n_z + 16
+    copies = 8 * n_ep + 4 * n_tp + 12 * n_z + 16
     scratch = [pltpu.VMEM(w.shape, bf16) for w in (eg, eu, ed)]
     scratch += [
         pltpu.VMEM((2, quarter, units), bf16),
@@ -490,10 +519,10 @@
         pltpu.VMEM((items, quarter), f32),
         pltpu.VMEM((n_tp, 2, n_z // 2 * sub, units), bf16),
         pltpu.VMEM((2, n_tp, n_z // 2 * sub, quarter), f32),
-        pltpu.VMEM((n_z, tokens, quarter), bf16),
-        pltpu.VMEM((n_z, tokens, quarter), bf16),
-        pltpu.VMEM((n_z - 1, tokens, quarter), bf16),
-        pltpu.VMEM((n_z - 1, tokens, quarter), bf16),
+        pltpu.VMEM((n_z, 2, tokens, quarter // 2), bf16),
+        pltpu.VMEM((n_z, 2, tokens, quarter // 2), bf16),
+        pltpu.VMEM((n_z - 1, 2, tokens, quarter // 2), bf16),
+        pltpu.VMEM((n_z - 1, 2, tokens, quarter // 2), bf16),
         pltpu.SemaphoreType.DMA((6,)),
         pltpu.SemaphoreType.DMA((copies,)),
         pltpu.SemaphoreType.DMA((copies,)),
@@ -570,7 +599,7 @@
     )
     for i, (src, dst) in enumerate(pairs):
         loads.append(pltpu.make_async_copy(src, dst, w_sem.at[i]))
-    for i in (5, 6, 0, 1, 2, 3, 7, 8, 9, 10):
+    for i in (5, 6, 7, 8, 0, 1, 2, 3, 9, 10):
         loads[i].start()
 
     def fetch(g):

time: 50.3 us -> 49.4 us (0.982)
  Pallas kernels: 48.9 us -> 47.9 us
    pallas_call x1, Pallas kernels: 42.2 us -> 41.4 us  [run_layer(): pl.pallas_call(functools.partial(layer_kernel, n_ep, n_tp), out_shape=jax...]
where the time goes in v5:
time: 49.4 us; the launch traced here: 49.2 us
  Pallas kernels  47.9 us (97%)
  between operations  0.68 us (1%)
  local copies, waits for them, and re-layouts  0.63 us (1%)
    pallas_call x1, Pallas kernels, run_layer(): pl.pallas_call(functools.partial(layer_kernel, n_ep, n_tp), out_shape=jax...  41.4 us
    pallas_call x1, Pallas kernels, run_attention(): pl.pallas_call(functools.partial(attention_kernel, cap), out_shape=(pltpu...  6.53 us

profile of v5, /device:TPU:0, one launch (start us, length us, event | category | flops | bytes accessed | tf_op | source)
XLA Modules:
  0.0 49.2 jit_solution(1177523254912422576)
XLA Ops:
  0.6 0.0 copy-start
  0.6 0.0 copy-start.1
  0.7 6.5 %shard_map.212 = (bf16[48,256]{1,0:T(8,128)(2,1)S(1)}, bf16[128,128]{1,0:T(8,128)(2,1)S(1)}, bf16[48,2048]{1,0:T(8,128)(2,1)S(1)}, bf16[256,2048]{1,0:T(8,128)(2,1)S(1)}, f32[48,1,128,256]{3,2,1,0:T(8,128)}) custom-call(bf16[48,2048]{1,0:T(8,128)(2,1)} %hidden_hbm.1, bf16[16,128]{1,0:T(8,128)(2,1)} %bitcast.15, f32[48,128]{1,0:T(8,128)} %shift_hbm.1, ...), custom_call_target="tpu_custom_call" | custom-call | tf_op jit(solution)/shard_map/pallas_call | solution.py:712
  7.2 0.0 copy-done
  7.2 0.0 copy-done.1
  7.2 41.4 %shard_map.213 = bf16[48,512]{1,0:T(8,128)(2,1)S(1)} custom-call(bf16[48,256]{1,0:T(8,128)(2,1)S(1)} %get-tuple-element.7.gated_ref, bf16[256,2048]{1,0:T(8,128)(2,1)S(1)} %get-tuple-element.8.outw_ref, bf16[48,2048]{1,0:T(8,128)(2,1)S(1)} %get-tuple-element.9.hid_ref, bf16[16,128]{1,0:T(8,128)(2,1)S(1)} %bitcast.10, bf16[16,128]{1,0:T(8,128)(2,1)S(1)} %bitcast.11, ...), custom_call_target="tpu_custom_call" | custom-call | tf_op jit(solution)/shard_map/pallas_call | solution.py:530
  48.6 0.6 %copy.24 = bf16[48,512]{1,0:T(8,128)(2,1)} copy(bf16[48,512]{1,0:T(8,128)(2,1)S(1)} %shard_map.213) | data formatting | bytes 98304
Async XLA Ops:
  0.6 6.6 %copy-start = (bf16[2048]{0:T(1024)(128)(2,1)S(1)}, bf16[2048]{0:T(1024)(128)(2,1)}, u32[]{:S(2)}) copy-start(bf16[2048]{0:T(1024)(128)(2,1)} %param.32) | copy-start | bytes 12292
  0.6 6.6 %copy-start.1 = (bf16[2048]{0:T(1024)(128)(2,1)S(1)}, bf16[2048]{0:T(1024)(128)(2,1)}, u32[]{:S(2)}) copy-start(bf16[2048]{0:T(1024)(128)(2,1)} %param.33) | copy-start | bytes 12292
